TPU v7x, 512 devices: a whole 4x8x8 slice. The times are simulated.
512 devices in a mesh: sp: 32 (over z, x), tp: 16 (over y, core).
Axes of the slice: x: 4, y: 8, z: 8, core: 2. Of those that a mesh axis runs over, the one named last changes fastest.
Arguments:
- residual: bfloat16 [6144, 2048], P(('sp', 'tp')), may hold values from -6 to 6
- query_a: bfloat16 [6144, 1536], P('sp', 'tp'), may hold values from -600 to 600
- query_b: bfloat16 [6144, 2560], P('sp', 'tp'), may hold values from -600 to 600
- latents: bfloat16 [6144, 512], P('sp'), may hold values from -6 to 6
- rope_key: bfloat16 [6144, 32], P('sp'), may hold values from -6 to 6
- key_up_a: bfloat16 [512, 1024], P(None, 'tp'), may hold values from -0.25 to 0.25
- value_up_a: bfloat16 [512, 1024], P(None, 'tp'), may hold values from -0.25 to 0.25
- key_up_b: bfloat16 [512, 2048], P(None, 'tp'), may hold values from -0.25 to 0.25
- value_up_b: bfloat16 [512, 2048], P(None, 'tp'), may hold values from -0.25 to 0.25
- out_proj_a: bfloat16 [1024, 2048], P('tp'), may hold values from -1.5 to 1.5
- out_proj_b: bfloat16 [2048, 2048], P('tp'), may hold values from -1.5 to 1.5
- norm_gain: float32 [2048], replicated, may hold values from 0.1 to 1.9
- routes: int32 [6144, 2], P('sp'), may hold values from 0 to 31, all different within a row; in each aligned block of 192 rows (0 to 191, 192 to 383, ...) at most 18 rows name the same one
- route_weights: float32 [6144, 2], P('sp'), may hold values from 0.2 to 1
- shared_gate: bfloat16 [2048, 2048], P(None, 'tp'), may hold values from -0.125 to 0.125
- shared_up: bfloat16 [2048, 2048], P(None, 'tp'), may hold values from -0.125 to 0.125
- shared_down: bfloat16 [2048, 2048], P('tp'), may hold values from -0.125 to 0.125
- expert_gate: bfloat16 [32, 2048, 2048], P('sp', None, 'tp'), may hold values from -0.125 to 0.125
- expert_up: bfloat16 [32, 2048, 2048], P('sp', None, 'tp'), may hold values from -0.125 to 0.125
- expert_down: bfloat16 [32, 2048, 2048], P('sp', 'tp'), may hold values from -0.125 to 0.125
Outputs:
- layer_out: bfloat16 [6144, 2048], P(('sp', 'tp'))
Inputs may be any that keep to these rules, and one draw needn't show every extreme that they name: `routes`: in each aligned block of 192 rows, no expert is named by more than 18 rows, a bound that some block reaches; a row names 2 different experts.
All inputs are finite; a program needn't handle non-finite values.
Results may differ from a plain program's by a relative error of at most 0.022.
The roundings to bfloat16 on the way count: a program that leaves them out, or rounds other values in their place, can miss the bound.
Values may be sent and summed in bfloat16 or wider, within the bound.
A program may use at most 64 MiB of HBM per device.

v0:
```python
import jax
import jax.numpy as jnp
from jax import lax
from jax.sharding import Mesh
from jax.sharding import PartitionSpec as P

DA = 64
VA = 64
DB = 128
VB = 128
ROPE = 32
TP = ("tp_0", "tp_1")
SP_TP = ("sp", "tp_0", "tp_1")


theta_base = 10000.0
norm_eps = 1e-06
very_low = -1e30


def sent_together(arrays, axis, dim, along):
    ends, at = ([], 0)
    for a in arrays[:-1]:
        at += a.shape[along]
        ends.append(at)
    both = jnp.concatenate(arrays, axis=along)
    return tuple(jnp.split(lax.all_gather(both, axis, axis=dim, tiled=True), ends, axis=along))


def cut_along(value, dim, length):
    shape = value.shape
    tiles = value.reshape(*shape[:dim], length, shape[dim] // length, *shape[dim + 1 :])
    return jnp.moveaxis(tiles, dim, 0)


def sum_at_owner(value, axis, dim):
    tiles = cut_along(value, dim, lax.axis_size(axis))
    arrived = lax.all_to_all(tiles, axis, split_axis=0, concat_axis=0, tiled=True)
    return arrived.astype(jnp.float32).sum(axis=0)


def whole_of(value, axes, dim):
    for axis in reversed(axes):
        value = lax.all_gather(value, axis, axis=dim, tiled=True)
    return value


def tables(positions, width):
    half = width // 2
    freqs = theta_base ** (-(2.0 * jnp.arange(half, dtype=jnp.float32)) / width)
    angles = positions.astype(jnp.float32)[:, None] * freqs[None, :]
    return (jnp.cos(angles), jnp.sin(angles))


def rotate(values, cosine, sine):
    half = values.shape[-1] // 2
    first = values[..., :half].astype(jnp.float32)
    second = values[..., half:].astype(jnp.float32)
    turned = jnp.concatenate(
        [first * cosine - second * sine, first * sine + second * cosine], axis=-1
    )
    return turned.astype(jnp.bfloat16)


def group_update(state, queries_nope, queries_rope, keys, values, rot_piece, mask, scale):
    top, total, weighted = state
    scores = jnp.einsum("qhd,khd->hqk", queries_nope, keys, preferred_element_type=jnp.float32)
    scores = scores + jnp.einsum(
        "qhr,kr->hqk", queries_rope, rot_piece, preferred_element_type=jnp.float32
    )
    scores = jnp.where(mask[None], scores * scale, very_low)
    new_top = jnp.maximum(top, jnp.max(scores, axis=-1))
    expo = jnp.where(mask[None], jnp.exp(scores - new_top[..., None]), 0.0)
    total = jnp.sum(expo, axis=-1)
    weighted = jnp.einsum(
        "hqk,khv->hqv", expo.astype(jnp.bfloat16), values, preferred_element_type=jnp.float32
    )
    return (new_top, total, weighted)


def empty_state(heads, rows, vsize):
    return (
        jnp.full((heads, rows), very_low, jnp.float32),
        jnp.zeros((heads, rows), jnp.float32),
        jnp.zeros((heads, rows, vsize), jnp.float32),
    )


def shards(
    residual,
    query_a,
    query_b,
    latents,
    rope_key,
    key_up_a,
    value_up_a,
    key_up_b,
    value_up_b,
    out_proj_a,
    out_proj_b,
    norm_gain,
    routes,
    route_weights,
    shared_gate,
    shared_up,
    shared_down,
    expert_gate,
    expert_up,
    expert_down,
):
    tok = query_a.shape[0]
    heads_a = key_up_a.shape[1] // DA
    heads_b = key_up_b.shape[1] // DB
    first_row = lax.axis_index("sp") * tok
    last_row = first_row + tok
    query_pos = first_row + jnp.arange(tok, dtype=jnp.int32)
    cosine, sine = tables(query_pos, ROPE)
    rot_key = rotate(rope_key, cosine, sine)
    shaped_a = query_a.reshape(tok, heads_a, DA + ROPE)
    shaped_b = query_b.reshape(tok, heads_b, DB + ROPE)
    nope_a = shaped_a[..., :DA]
    nope_b = shaped_b[..., :DB]
    turned_a = rotate(shaped_a[..., DA:], cosine[:, None, :], sine[:, None, :])
    turned_b = rotate(shaped_b[..., DB:], cosine[:, None, :], sine[:, None, :])
    scale_a = (DA + ROPE) ** (-0.5)
    scale_b = (DB + ROPE) ** (-0.5)

    def attend(state, keys_a, values_a, keys_b, values_b, rot_piece, key_pos):
        count = keys_a.shape[0]
        mask = key_pos[None, :] <= query_pos[:, None]
        state_a = group_update(
            state[0],
            nope_a,
            turned_a,
            keys_a.reshape(count, heads_a, DA),
            values_a.reshape(count, heads_a, VA),
            rot_piece,
            mask,
            scale_a,
        )
        state_b = group_update(
            state[1],
            nope_b,
            turned_b,
            keys_b.reshape(count, heads_b, DB),
            values_b.reshape(count, heads_b, VB),
            rot_piece,
            mask,
            scale_b,
        )
        return (state_a, state_b)

    start_state = (empty_state(heads_a, tok, VA), empty_state(heads_b, tok, VB))
    keys_a = jnp.dot(latents, key_up_a, preferred_element_type=jnp.float32).astype(jnp.bfloat16)
    values_a = jnp.dot(latents, value_up_a, preferred_element_type=jnp.float32).astype(jnp.bfloat16)
    keys_b = jnp.dot(latents, key_up_b, preferred_element_type=jnp.float32).astype(jnp.bfloat16)
    values_b = jnp.dot(latents, value_up_b, preferred_element_type=jnp.float32).astype(jnp.bfloat16)
    keys_a, values_a, keys_b, values_b = (keys_a, values_a, keys_b, values_b)
    piece = sent_together((keys_a, values_a, keys_b, values_b, rot_key), "sp", 0, 1)
    key_pos = jnp.arange(piece[0].shape[0], dtype=jnp.int32)

    def compute(inner):
        return attend(inner, piece[0], piece[1], piece[2], piece[3], piece[4], key_pos)

    state = lax.cond(jnp.int32(0) < last_row, compute, lambda inner: inner, start_state)
    heads_out_a = (state[0][2] / state[0][1][..., None]).astype(jnp.bfloat16)
    heads_out_b = (state[1][2] / state[1][1][..., None]).astype(jnp.bfloat16)
    proj_a = out_proj_a.reshape(heads_a, VA, out_proj_a.shape[1])
    proj_b = out_proj_b.reshape(heads_b, VB, out_proj_b.shape[1])
    term = jnp.einsum("hqv,hvd->qd", heads_out_a, proj_a, preferred_element_type=jnp.float32)
    mixed = sum_at_owner(
        (
            term
            + jnp.einsum("hqv,hvd->qd", heads_out_b, proj_b, preferred_element_type=jnp.float32)
        ).astype(jnp.bfloat16),
        TP,
        0,
    )
    hidden_state = (residual.astype(jnp.float32) + mixed).astype(jnp.bfloat16)
    wide = hidden_state.astype(jnp.float32)
    normed = (
        wide * lax.rsqrt(jnp.mean(wide * wide, axis=-1, keepdims=True) + norm_eps) * norm_gain
    ).astype(jnp.bfloat16)
    whole_rows = whole_of(normed, TP, 0)
    shared_act = (
        jax.nn.silu(jnp.dot(whole_rows, shared_gate, preferred_element_type=jnp.float32))
        * jnp.dot(whole_rows, shared_up, preferred_element_type=jnp.float32)
    ).astype(jnp.bfloat16)
    experts = lax.axis_size("sp")
    topk = routes.shape[1]
    capacity = max(2, 3 * tok * topk // (2 * experts))
    flat = routes.reshape(-1)
    onehot = (flat[:, None] == jnp.arange(experts, dtype=jnp.int32)[None, :]).astype(jnp.int32)
    before = jnp.cumsum(onehot, axis=0) - onehot
    rank = jnp.sum(before * onehot, axis=1)
    slots = (flat * capacity + rank).reshape(tok, topk)
    placing = jnp.sum(
        (
            slots[:, :, None] == jnp.arange(experts * capacity, dtype=jnp.int32)[None, None, :]
        ).astype(jnp.bfloat16),
        axis=1,
    )
    outgoing = jnp.einsum(
        "rs,rd->sd", placing, whole_rows, preferred_element_type=jnp.float32
    ).astype(jnp.bfloat16)
    outgoing = outgoing.reshape(experts, capacity, whole_rows.shape[1])
    gate_w = expert_gate[0]
    up_w = expert_up[0]
    down_w = expert_down[0]
    arrived = lax.all_to_all(outgoing, "sp", split_axis=0, concat_axis=0, tiled=True)
    sources, items, width = arrived.shape
    rows_in = arrived.reshape(sources * items, width)
    act = (
        jax.nn.silu(jnp.dot(rows_in, gate_w, preferred_element_type=jnp.float32))
        * jnp.dot(rows_in, up_w, preferred_element_type=jnp.float32)
    ).astype(jnp.bfloat16)
    part = jnp.dot(act, down_w, preferred_element_type=jnp.float32).astype(jnp.bfloat16)
    back = lax.all_to_all(
        part.reshape(sources, items, down_w.shape[1]), "sp", split_axis=0, concat_axis=0, tiled=True
    )
    back_flat = back.reshape(experts * capacity, back.shape[2])
    term = jnp.dot(shared_act, shared_down, preferred_element_type=jnp.float32)
    picked = jnp.take(back_flat, slots, axis=0).astype(jnp.float32)
    moe = sum_at_owner(
        (term + jnp.sum(picked * route_weights[..., None], axis=1)).astype(jnp.bfloat16), TP, 0
    )
    return (hidden_state.astype(jnp.float32) + moe).astype(jnp.bfloat16)


def solution(mesh):
    torus = Mesh(mesh.devices.reshape(mesh.shape["sp"], 8, 2), ("sp", "tp_0", "tp_1"))
    in_specs = (
        P(SP_TP, None),
        P("sp", TP),
        P("sp", TP),
        P("sp", None),
        P("sp", None),
        P(None, TP),
        P(None, TP),
        P(None, TP),
        P(None, TP),
        P(TP, None),
        P(TP, None),
        P(),
        P("sp", None),
        P("sp", None),
        P(None, TP),
        P(None, TP),
        P(TP, None),
        P("sp", None, TP),
        P("sp", None, TP),
        P("sp", TP, None),
    )
    out_specs = P(SP_TP, None)
    return jax.shard_map(
        shards, mesh=torus, in_specs=in_specs, out_specs=out_specs, check_vma=False
    )
```

profile of v0, /device:TPU:1, one launch (start us, length us, event | category | flops | bytes accessed | tf_op | source)
XLA Modules:
  0.0 425.2 jit_solution(7554255772300763512)
XLA Ops:
  15.5 97.3 %all-gather.3.cloned.1.call-done = bf16[6144,416]{1,0:T(8,128)(2,1)} async-done(((bf16[192,416]{1,0:T(8,128)(2,1)}), bf16[6144,416]{1,0:T(8,128)(2,1)}) %all-gather.3.cloned.1.call-update) | async-done | bytes 5111824 | tf_op jit(solution)/shard_map/all_gather | solution.py:27
  112.8 19.2 %conditional.1 = (f32[1,192]{1,0:T(1,128)S(1)}, f32[1,192,64]{1,2,0:T(8,128)S(1)}, f32[1,192]{1,0:T(1,128)S(1)}, f32[1,192,128]{2,1,0:T(8,128)S(1)}) conditional(s32[]{:T(128)} %convert_element_type.127, () %tuple.13, (s32[6144]{0:T(1024)S(1)}, s32[]{:T(128)}, s32[192]{0:T(256)S(1)}, bf16[192,1,96]{2,0,1:T(8,128)(2,1)}, bf16[6144,416]{1,0:T(8,128)(2,1)}, ...), branch_computations={%region_0.0_spmd, %region_1.6_spmd} | conditional | flops 1086455552 | bytes 90389920 | solution.py:165
  113.9 2.2 convolution_bitcast_fusion.1
  116.1 5.0 %fusion.95 = (f32[192]{0:T(256)S(1)}, f32[1,192,6144]{2,1,0:T(8,128)}) fusion(f32[1,192,6144]{2,1,0:T(8,128)S(1)} %convolution_bitcast_fusion.1, bf16[192,1,32]{0,2,1:T(8,128)(2,1)S(1)} %get-tuple-element.41, bf16[6144,416]{1,0:T(8,128)(2,1)} %get-tuple-element.38, s32[192]{0:T(256)S(1)} %broadcast_add_fusion, s32[6144]{0:T(1024)S(1)} %get-tuple-element.34), kind=kOutput, calls=%fused_computation.137 | convolution fusion | flops 81395520 | bytes 11048448 | tf_op jit(solution)/shard_map/cond/branch_1_fun/qhr,kr->hqk/dot_general | solution.py:68
  121.2 2.4 convolution_bitcast_fusion.3
  123.6 3.4 fusion.96
  129.9 2.1 fusion.7
  134.1 8.0 %all-to-all-start = ((bf16[16,12,2048]{2,1,0:T(8,128)(2,1)}), bf16[16,12,2048]{2,1,0:T(8,128)(2,1)S(1)}, u32[]{:S(2)}, u32[]{:S(2)}) async-start(bf16[16,12,2048]{2,1,0:T(8,128)(2,1)} %reshape.335), calls=%async_computation | async-start | bytes 2097152 | tf_op jit(solution)/shard_map/all_to_all | solution.py:38
  144.1 25.9 %all-to-all-done = bf16[16,12,2048]{2,1,0:T(8,128)(2,1)S(1)} async-done(((bf16[16,12,2048]{2,1,0:T(8,128)(2,1)}), bf16[16,12,2048]{2,1,0:T(8,128)(2,1)S(1)}, u32[]{:S(2)}, u32[]{:S(2)}) %all-to-all-start) | async-done | bytes 786464 | tf_op jit(solution)/shard_map/all_to_all | solution.py:38
  170.4 1.9 all-gather
  172.4 20.6 %all_gather.11 = bf16[192,2048]{1,0:T(8,128)(2,1)S(1)} all-gather(bf16[24,2048]{1,0:T(8,128)(2,1)S(1)} %reshape.353), channel_id=1, replica_groups=mesh['sp'=32,'tp_0'=8,'tp_1'=2] {'tp_0'}, dimensions={0}, use_global_device_ids=true | all-gather | bytes 884736 | tf_op jit(solution)/shard_map/all_gather | solution.py:44
  194.7 2.4 reshape.337
  197.1 71.6 %all_to_all.20 = bf16[32,18,2048]{2,1,0:T(8,128)(2,1)} all-to-all(bf16[32,18,2048]{2,1,0:T(8,128)(2,1)} %reshape.337), channel_id=1, replica_groups=mesh['sp'=32,'tp_0'=8,'tp_1'=2] {'sp'}, dimensions={0} | all-to-all | bytes 4718592 | tf_op jit(solution)/shard_map/all_to_all | solution.py:210
  268.7 2.9 reshape.338
  273.5 5.0 %convolution_convert_fusion = bf16[576,2048]{1,0:T(8,128)(2,1)} fusion(bf16[576,2048]{1,0:T(8,128)(2,1)S(1)} %reshape.338, bf16[1,128,2048]{2,1,0:T(8,128)(2,1)S(1)} %copy-done, bf16[1,2048,128]{2,1,0:T(8,128)(2,1)} %param.40, f32[576,128]{1,0:T(8,128)S(1)} %fusion.42), kind=kOutput, calls=%fused_computation.40 | convolution fusion | flops 605601792 | bytes 6062080 | tf_op jit(solution)/shard_map/dot_general | solution.py:217
  278.6 4.4 %reshape.339 = bf16[32,18,2048]{2,1,0:T(8,128)(2,1)} reshape(bf16[576,2048]{1,0:T(8,128)(2,1)} %convolution_convert_fusion) | data formatting | bytes 4718592 | tf_op jit(solution)/shard_map/reshape | solution.py:219
  283.0 7.4 %all-to-all-start.2 = ((bf16[32,18,2048]{2,1,0:T(8,128)(2,1)}), bf16[32,18,2048]{2,1,0:T(8,128)(2,1)}, u32[]{:S(2)}, u32[]{:S(2)}) async-start(bf16[32,18,2048]{2,1,0:T(8,128)(2,1)} %reshape.339), calls=%async_computation.2 | async-start | bytes 6291456 | tf_op jit(solution)/shard_map/all_to_all | solution.py:218
  291.4 64.5 %all-to-all-done.2 = bf16[32,18,2048]{2,1,0:T(8,128)(2,1)} async-done(((bf16[32,18,2048]{2,1,0:T(8,128)(2,1)}), bf16[32,18,2048]{2,1,0:T(8,128)(2,1)}, u32[]{:S(2)}, u32[]{:S(2)}) %all-to-all-start.2) | async-done | bytes 2359328 | tf_op jit(solution)/shard_map/all_to_all | solution.py:218
  355.9 2.9 reshape.340
  358.9 3.1 gather_fusion
  362.0 3.8 reshape.343
  365.8 7.6 %multiply_reduce_fusion = f32[192,2048]{1,0:T(8,128)S(1)} fusion(bf16[192,2,2048]{2,1,0:T(2,128)(2,1)} %reshape.343, pred[192,2]{1,0:T(8,128)(4,1)S(1)} %copy.94, f32[192,2]{1,0:T(8,128)S(1)} %copy.96), kind=kLoop, calls=%fused_computation.38 | loop fusion | flops 2752512 | bytes 3147648 | tf_op jit(solution)/shard_map/reduce_sum | solution.py:225
  373.4 2.7 fusion.35
  377.4 40.0 %all_to_all.21 = bf16[16,12,2048]{2,1,0:T(8,128)(2,1)S(1)} all-to-all(bf16[16,12,2048]{2,1,0:T(8,128)(2,1)S(1)} %reshape.341), channel_id=1, replica_groups=mesh['sp'=32,'tp_0'=8,'tp_1'=2] {'tp_0','tp_1'}, dimensions={0} | all-to-all | bytes 1572864 | tf_op jit(solution)/shard_map/all_to_all | solution.py:38
  (93 shorter events, 23.9 us)
Async XLA Ops:
  6.5 267.0 %copy-start = (bf16[1,128,2048]{2,1,0:T(8,128)(2,1)S(1)}, bf16[1,128,2048]{2,1,0:T(8,128)(2,1)}, u32[]{:S(2)}) copy-start(bf16[1,128,2048]{2,1,0:T(8,128)(2,1)} %param.41) | copy-start | bytes 1572868
  6.5 106.3 %all-gather.3.cloned.1.call-start = ((), (), s32[]{:S(2)}) async-start(), calls=%async_computation.4 | async-start | bytes 6488064 | tf_op jit(solution)/shard_map/all_gather | solution.py:27
  112.8 19.2 %copy-start.7 = (bf16[64,2048]{1,0:T(8,128)(2,1)S(1)}, bf16[64,2048]{1,0:T(8,128)(2,1)}, u32[]{:S(2)}) copy-start(bf16[64,2048]{1,0:T(8,128)(2,1)} %param.31) | copy-start | bytes 786436
  112.8 19.7 %copy-start.4 = (bf16[128,2048]{1,0:T(8,128)(2,1)S(1)}, bf16[128,2048]{1,0:T(8,128)(2,1)}, u32[]{:S(2)}) copy-start(bf16[128,2048]{1,0:T(8,128)(2,1)} %param.32) | copy-start | bytes 1572868
  116.1 5.0 %copy-start.6 = (bf16[192,1,96]{2,0,1:T(8,128)(2,1)S(1)}, bf16[192,1,96]{2,0,1:T(8,128)(2,1)}, u32[]{:S(2)}) copy-start(bf16[192,1,96]{2,0,1:T(8,128)(2,1)} %get-tuple-element.77) | copy-start | bytes 110596 | tf_op jit(solution)/shard_map/cond
  121.2 5.8 %slice-start = ((s8[4718592]{0:T(1024)(128)(4,1)}), s8[4194304]{0:T(1024)(128)(4,1)S(1)}, s32[]{:S(2)}) async-start(s8[4718592]{0:T(1024)(128)(4,1)} %bitcast.117), calls=%async_computation.5 | async-start | bytes 8388608 | tf_op jit(solution)/shard_map/cond
  121.2 5.8 %slice-start.2 = ((s8[6291456]{0:T(1024)(128)(4,1)}), s8[4194304]{0:T(1024)(128)(4,1)S(1)}, s32[]{:S(2)}) async-start(s8[6291456]{0:T(1024)(128)(4,1)} %bitcast.119), calls=%async_computation.7 | async-start | bytes 8388608 | tf_op jit(solution)/shard_map/cond
  123.6 3.4 slice-start.1
  123.6 3.4 slice-start.3
  132.0 10.0 %copy-start.10 = (s32[192,2]{0,1:T(2,128)S(1)}, s32[192,2]{0,1:T(2,128)}, u32[]{:S(2)}) copy-start(s32[192,2]{0,1:T(2,128)} %param.34) | copy-start | bytes 4612
  132.4 37.7 %copy-start.8 = (bf16[12,2048]{1,0:T(8,128)(2,1)S(1)}, bf16[12,2048]{1,0:T(8,128)(2,1)}, u32[]{:S(2)}) copy-start(bf16[12,2048]{1,0:T(8,128)(2,1)} %param.22) | copy-start | bytes 147460
  132.5 37.9 %copy-start.9 = (f32[2048]{0:T(1024)S(1)}, f32[2048]{0:T(1024)}, u32[]{:S(2)}) copy-start(f32[2048]{0:T(1024)} %param.33) | copy-start | bytes 24580
  134.1 35.9 %all-to-all-start = ((bf16[16,12,2048]{2,1,0:T(8,128)(2,1)}), bf16[16,12,2048]{2,1,0:T(8,128)(2,1)S(1)}, u32[]{:S(2)}, u32[]{:S(2)}) async-start(bf16[16,12,2048]{2,1,0:T(8,128)(2,1)} %reshape.335), calls=%async_computation | async-start | bytes 2097152 | tf_op jit(solution)/shard_map/all_to_all | solution.py:38
  193.0 0.9 copy-start.1
  278.6 12.3 %copy-start.11 = (f32[192,2]{0,1:T(2,128)S(1)}, f32[192,2]{0,1:T(2,128)}, u32[]{:S(2)}) copy-start(f32[192,2]{0,1:T(2,128)} %param.35) | copy-start | bytes 4612
  278.6 12.4 %copy-start.2 = (bf16[192,2048]{1,0:T(8,128)(2,1)S(1)}, bf16[192,2048]{1,0:T(8,128)(2,1)}, u32[]{:S(2)}) copy-start(bf16[192,2048]{1,0:T(8,128)(2,1)} %copy-done.1) | copy-start | bytes 2359300
  278.6 12.5 %copy-start.5 = (bf16[2048,128]{1,0:T(8,128)(2,1)S(1)}, bf16[2048,128]{1,0:T(8,128)(2,1)}, u32[]{:S(2)}) copy-start(bf16[2048,128]{1,0:T(8,128)(2,1)} %param.36) | copy-start | bytes 1572868
  283.0 73.0 %all-to-all-start.2 = ((bf16[32,18,2048]{2,1,0:T(8,128)(2,1)}), bf16[32,18,2048]{2,1,0:T(8,128)(2,1)}, u32[]{:S(2)}, u32[]{:S(2)}) async-start(bf16[32,18,2048]{2,1,0:T(8,128)(2,1)} %reshape.339), calls=%async_computation.2 | async-start | bytes 6291456 | tf_op jit(solution)/shard_map/all_to_all | solution.py:218
  362.0 11.4 %copy-start.3 = (bf16[192,2048]{1,0:T(8,128)(2,1)S(1)}, bf16[192,2048]{1,0:T(8,128)(2,1)}, u32[]{:S(2)}) copy-start(bf16[192,2048]{1,0:T(8,128)(2,1)} %copy-done.1) | copy-start | bytes 2359300
Sparse Core Ops, SparseCore 0:
  13.6 99.2 all-gather.2
where the time goes:
time: 426 us; the launch traced here: 425 us
  waiting for transfers between devices  188 us (44%)
  blocking collectives  134 us (31%)
  matrix products  32 us (8%)
  local copies, waits for them, and re-layouts  27.9 us (7%)
  starting transfers between devices  15.4 us (4%)
  other arithmetic  14 us (3%)
  between operations  13.7 us (3%)
    all_gather x1, waiting for transfers between devices, sent_together(): lax.all_gather(both, axis, axis=dim, tiled=True)  97.3 us
    all_to_all x1, blocking collectives, shards(): lax.all_to_all(outgoing, 'sp', split_axis=0, concat_axis=0, tiled=True)  71.6 us
    all_to_all x1, waiting for transfers between devices, shards(): lax.all_to_all(part.reshape(sources, items, down_w.shape[1]), 'sp', split...  64.5 us
    all_to_all x1, blocking collectives, sum_at_owner(): lax.all_to_all(tiles, axis, split_axis=0, concat_axis=0, tiled=True)  40 us
    all_to_all x1, waiting for transfers between devices, sum_at_owner(): lax.all_to_all(tiles, axis, split_axis=0, concat_axis=0, tiled=True)  25.9 us
    all_gather x2, blocking collectives, whole_of(): value = lax.all_gather(value, axis, axis=dim, tiled=True)  22.5 us
  transfers between devices with their start and end apart: 3, of which 3 were waited for; matrix products, arithmetic and copies ran while one was open for 1% of the time, Pallas kernels for 0%

commit v1 on v0

v1 whole, which is shorter than its diff:
```python
import functools

import jax
import jax.numpy as jnp
from jax import lax
from jax.experimental import pallas as pl
from jax.experimental.pallas import tpu as pltpu
from jax.sharding import Mesh
from jax.sharding import PartitionSpec as P

DA = 64
VA = 64
DB = 128
VB = 128
ROPE = 32
TOK = 192
D = 2048
W = 128
CAP = 18
CAPP = 24
NZ, NX, NY, NC = 4 * 2, 4, 8, 2
NSP = NZ * NX
NTP = NY * NC
ROWS = NSP * CAP
PROWS = NSP * CAPP
HALF = ROWS // 2
OWN = TOK // NTP
OWNP = 16
SP = ("z", "x")
TP = ("y", "c")
ALL = ("z", "x", "y", "c")
MESH_ID = pl.DeviceIdType.MESH
F32 = jnp.float32
BF16 = jnp.bfloat16
FAR_FIRST = (4, 3, 5, 2, 6, 1, 7, 0)

theta_base = 10000.0
norm_eps = 1e-06
very_low = -1e30


def fdot(a, b):
    return jnp.dot(a, b, preferred_element_type=F32)


def rcopy(src, dst, ssem, rsem, dev):
    return pltpu.make_async_remote_copy(
        src_ref=src, dst_ref=dst, send_sem=ssem, recv_sem=rsem, device_id=dev, device_id_type=MESH_ID
    )


def iota(shape, dim):
    return lax.broadcasted_iota(jnp.int32, shape, dim)


def onehot(cond):
    return jnp.where(cond, 1.0, 0.0).astype(BF16)


def lanes(index, width):
    return pl.ds(pl.multiple_of(index * width, 128), width)


def post_kernel(
    heads_a, heads_b, resid, gain, routes, routes_t, rw,
    oa_h, ob_h, sg_h, su_h, sd_h, eg_h, eu_h, ed_h,
    out,
    oa, ob, sgu, sd, egu, ed,
    r_r, own_d, po_d, pi_d, sb_d, rb_d,
    hs, hfull, normed,
    po_s, pi_s, sb_s, rb_s, own_s,
    f_s, f_r, comp, expd, g, hacc,
    own_i, po_i, pi_i, isb, irb, j_r, l_s, l_r,
    w_sem, r_ss, r_rs, pd_ss, pd_rs, d_ss, d_rs, e_ss, e_rs, ef_ss, ef_rs,
    ps_ss, ps_rs, s_ss, s_rs, f_ss, f_rs, g_ss, g_rs, gf_ss, gf_rs, go_ss, go_rs,
    pp_ss, pp_rs, i_ss, i_rs, j_ss, j_rs, l_ss, l_rs,
):
    z, x, y, c = (lax.axis_index(a) for a in ALL)
    t = y * NC + c
    sp = z * NX + x
    oc = 1 - c
    partner = (z, x, y, oc)

    def ydev(yy):
        return (z, x, yy, c)

    def tdev(tt):
        return (z, x, tt // NC, lax.rem(tt, NC))

    def sdev(ss):
        return (ss // NX, lax.rem(ss, NX), y, c)

    def yoff(off):
        return lax.rem(y + off, NY)

    weights = [
        (oa_h, oa), (ob_h, ob), (sg_h, sgu.at[:, 0:W]), (su_h, sgu.at[:, W:2 * W]), (sd_h, sd),
        (eg_h, egu.at[:, 0:W]), (eu_h, egu.at[:, W:2 * W]), (ed_h, ed),
    ]
    loads = [pltpu.make_async_copy(a, b, w_sem.at[i]) for i, (a, b) in enumerate(weights)]
    for load in loads:
        load.start()

    barrier = pltpu.get_barrier_semaphore()

    def greet_t(k, _):
        pl.semaphore_signal(barrier, inc=1, device_id=tdev(lax.rem(t + k, NTP)), device_id_type=MESH_ID)
        return 0

    def greet_s(k, _):
        pl.semaphore_signal(barrier, inc=1, device_id=sdev(lax.rem(sp + k, NSP)), device_id_type=MESH_ID)
        return 0

    lax.fori_loop(1, NTP, greet_t, 0)
    lax.fori_loop(1, NSP, greet_s, 0)

    names = onehot((iota((TOK, 128), 1) == routes[:, 0:1]) | (iota((TOK, 128), 1) == routes[:, 1:2]))
    lower = onehot(iota((TOK, TOK), 0) > iota((TOK, TOK), 1))
    before = fdot(lower, names)
    names_t = onehot((iota((128, TOK), 0) == routes_t[0:1, :]) | (iota((128, TOK), 0) == routes_t[1:2, :]))
    upper = onehot(iota((TOK, TOK), 0) < iota((TOK, TOK), 1))
    before_t = fdot(names_t, upper)

    def slot_col(k):
        rank = jnp.sum(jnp.where(iota((TOK, 128), 1) == routes[:, k:k + 1], before, 0.0), axis=1, keepdims=True)
        return routes[:, k:k + 1] * CAPP + rank.astype(jnp.int32)

    def slot_row(k):
        rank = jnp.sum(jnp.where(iota((128, TOK), 0) == routes_t[k:k + 1, :], before_t, 0.0), axis=0, keepdims=True)
        return routes_t[k:k + 1, :] * CAPP + rank.astype(jnp.int32)

    i_col = iota((ROWS, 1), 0)
    comp[...] = onehot(iota((ROWS, PROWS), 1) == i_col + (CAPP - CAP) * ((i_col * 3641) >> 16))
    j_col = iota((PROWS, 1), 0)
    j_q = (j_col * 2731) >> 16
    j_r0 = j_col - CAPP * j_q
    expd[...] = onehot(iota((PROWS, ROWS), 1) == jnp.where(j_r0 < CAP, CAP * j_q + j_r0, -1))

    loads[0].wait()
    loads[1].wait()
    pl.semaphore_wait(barrier, NTP - 1 + NSP - 1)

    def resid_copy(k, to):
        tt = lax.rem(t + k, NTP) if to else lax.rem(t + NTP - k, NTP)
        return rcopy(resid.at[:, lanes(tt if to else t, W)], r_r.at[t if to else tt], r_ss.at[k], r_rs.at[k], tdev(tt))

    def resid_send(k, _):
        resid_copy(k, True).start()
        return 0

    r_r[t] = resid[:, lanes(t, W)]

    def pair_out(value, off, own, po, pi, ss, rs):
        left, right = value[:, 0:W], value[:, W:2 * W]
        own[off] = jnp.where(c == 0, left, right)
        po[off] = jnp.where(c == 0, right, left).astype(BF16)
        rcopy(po.at[off], pi.at[off], ss.at[off], rs.at[off], partner).start()

    def pair_wait(off, po, pi, ss, rs):
        rcopy(po.at[off], pi.at[off], ss.at[off], rs.at[off], partner).wait()

    def y_copy(off, sb, rb, ss, rs):
        return rcopy(sb.at[off], rb.at[off], ss.at[off], rs.at[off], ydev(yoff(off)))

    def scatter_start(cols, own, po, pi, sb, rb, pss, prs, ss, rs, lead=3):
        for n in range(NY + lead):
            if n < NY:
                off = FAR_FIRST[n]
                pair_out(cols(yoff(off)), off, own, po, pi, pss, prs)
            if n >= lead:
                off = FAR_FIRST[n - lead]
                pair_wait(off, po, pi, pss, prs)
                if off:
                    sb[off] = (own[off] + pi[off].astype(F32)).astype(BF16)
                    y_copy(off, sb, rb, ss, rs).start()

    def scatter_end(own, pi, sb, rb, ss, rs):
        total = own[0] + pi[0].astype(F32)
        for off in range(1, NY):
            y_copy(off, sb, rb, ss, rs).wait()
            total = total + rb[off].astype(F32)
        return total

    def head_cols(yy):
        cut = lanes(yy, 2 * W)
        return fdot(heads_a[...], oa[:, cut]) + fdot(heads_b[...], ob[:, cut])

    scatter_start(head_cols, own_d, po_d, pi_d, sb_d, rb_d, pd_ss, pd_rs, d_ss, d_rs)
    lax.fori_loop(1, NTP, resid_send, 0)

    def resid_wait(k, _):
        resid_copy(k, False).wait()
        return 0

    mixed = scatter_end(own_d, pi_d, sb_d, rb_d, d_ss, d_rs)
    lax.fori_loop(1, NTP, resid_wait, 0)
    i12 = iota((TOK, 1), 0)
    pick12 = onehot(iota((TOK, NTP * OWNP), 1) == i12 + (OWNP - OWN) * ((i12 * 5462) >> 16))
    resid_cols = fdot(pick12, r_r[...].reshape(NTP * OWNP, W))
    hs[...] = (resid_cols + mixed).astype(BF16)

    hfull[:, lanes(t, W)] = hs[...]

    def e_copy(off):
        return rcopy(hs, hfull.at[:, lanes(t, W)], e_ss.at[off], e_rs.at[off], ydev(yoff(off)))

    def e_got(off):
        src = lanes(lax.rem(y + NY - off, NY) * NC + c, W)
        return rcopy(hs, hfull.at[:, src], e_ss.at[off], e_rs.at[off], ydev(yoff(off)))

    def e_fwd(off, core):
        win = hfull.at[:, lanes(lax.rem(y + NY - off, NY) * NC + core, W)]
        return rcopy(win, win, ef_ss.at[off], ef_rs.at[off], partner)

    for off in FAR_FIRST[:-1]:
        e_copy(off).start()
    e_fwd(0, c).start()
    for off in (1, 7, 2, 6, 3, 5, 4):
        e_got(off).wait_recv()
        e_fwd(off, c).start()
    for off in range(NY):
        e_fwd(off, oc).wait_recv()

    def norm_rows(b, _):
        rows = pl.ds(pl.multiple_of(b * 16, 16), 16)
        wide = hfull[rows, :].astype(F32)
        mean = jnp.mean(wide * wide, axis=-1, keepdims=True)
        normed[rows, :] = (wide * lax.rsqrt(mean + norm_eps) * gain[...]).astype(BF16)
        return 0

    lax.fori_loop(0, TOK // 16, norm_rows, 0)

    place = onehot((iota((PROWS, TOK), 0) == slot_row(0)) | (iota((PROWS, TOK), 0) == slot_row(1)))
    f_s[...] = fdot(place, normed[:, lanes(t, W)]).reshape(NSP, CAPP, W).astype(BF16)
    f_r[sp] = f_s[sp]

    def sp_copy(k, src, dst, ss, rs, to):
        peer = lax.rem(sp + k, NSP) if to else lax.rem(sp + NSP - k, NSP)
        return rcopy(src.at[peer], dst.at[sp if to else peer], ss.at[k], rs.at[k], sdev(peer))

    def f_send(k, _):
        sp_copy(k, f_s, f_r, f_ss, f_rs, True).start()
        return 0

    def f_wait(k, _):
        sp_copy(k, f_s, f_r, f_ss, f_rs, False).wait()
        return 0

    lax.fori_loop(1, NSP, f_send, 0)

    for load in loads[2:]:
        load.wait()
    both = fdot(normed[...], sgu[...])
    gate, up = both[:, 0:W], both[:, W:2 * W]
    shared_act = (gate / (1.0 + jnp.exp(-gate)) * up).astype(BF16)

    def shared_cols(yy):
        return fdot(shared_act, sd[:, lanes(yy, 2 * W)])

    scatter_start(shared_cols, own_s, po_s, pi_s, sb_s, rb_s, ps_ss, ps_rs, s_ss, s_rs)

    lax.fori_loop(1, NSP, f_wait, 0)
    g[y, :, lanes(c, W)] = fdot(comp[...], f_r[...].astype(F32).reshape(PROWS, W).astype(BF16)).astype(BF16)

    def ok_g(d, k, h):
        return k < 4 or h == d

    def ysrc(d, k):
        return lax.rem(y + NY - k, NY) if d == 0 else lax.rem(y + k, NY)

    def ydst(d):
        return ydev(lax.rem(y + 1, NY) if d == 0 else lax.rem(y + NY - 1, NY))

    def g_win(yy, h, core):
        return g.at[yy, pl.ds(h * HALF, HALF), lanes(core, W)]

    def g_send(d, k, h):
        win = g_win(ysrc(d, k - 1), h, c)
        return rcopy(win, win, g_ss.at[d, k - 1, h], g_rs.at[d, k - 1, h], ydst(d))

    def g_got(d, k, h):
        win = g_win(ysrc(d, k), h, c)
        return rcopy(win, win, g_ss.at[d, k - 1, h], g_rs.at[d, k - 1, h], ydst(d))

    def g_fwd(d, k, h, core):
        win = g_win(ysrc(d, k), h, core)
        return rcopy(win, win, gf_ss.at[d, k - 1, h], gf_rs.at[d, k - 1, h], partner)

    def g_own(core):
        win = g.at[y, :, lanes(core, W)]
        return rcopy(win, win, go_ss, go_rs, partner)

    for h in range(2):
        for d in range(2):
            g_send(d, 1, h).start()
    g_own(c).start()

    def gate_up(yy, first=False):
        value = fdot(g[yy], egu[pl.ds(pl.multiple_of(yy * 2 * W, 2 * W), 2 * W), :])
        hacc[...] = value if first else hacc[...] + value

    for k in range(1, 5):
        for h in range(2):
            for d in range(2):
                if ok_g(d, k, h):
                    g_got(d, k, h).wait_recv()
                    if k < 4 and ok_g(d, k + 1, h):
                        g_send(d, k + 1, h).start()
                    g_fwd(d, k, h, c).start()
        if k == 1:
            g_own(oc).wait_recv()
            gate_up(y, True)
        else:
            for d in range(2):
                for h in range(2):
                    g_fwd(d, k - 1, h, oc).wait_recv()
                gate_up(ysrc(d, k - 1))
    g_fwd(0, 4, 0, oc).wait_recv()
    g_fwd(1, 4, 1, oc).wait_recv()
    gate_up(yoff(4))
    gate, up = hacc[:, 0:W], hacc[:, W:2 * W]
    act = (gate / (1.0 + jnp.exp(-gate)) * up).astype(BF16)

    def i_pair(off):
        pair_out(fdot(act, ed[:, lanes(yoff(off), 2 * W)]), off, own_i, po_i, pi_i, pp_ss, pp_rs)

    def i_copy(d, k, h):
        return rcopy(isb.at[d, k - 1, h], irb.at[d, k - 1, h], i_ss.at[d, k - 1, h], i_rs.at[d, k - 1, h], ydst(d))

    def i_step(k):
        for h in range(2):
            for d in range(2):
                if k > 1 or h == d:
                    off = (5 - k) if d == 0 else (3 + k)
                    rows = pl.ds(h * HALF, HALF)
                    total = own_i[off, rows, :] + pi_i[off, rows, :].astype(F32)
                    if k > 2 or (k == 2 and h == d):
                        i_copy(d, k - 1, h).wait_recv()
                        total = total + irb[d, k - 2, h].astype(F32)
                    isb[d, k - 1, h] = total.astype(BF16)
                    i_copy(d, k, h).start()

    i_pair(4)
    i_pair(3)
    i_pair(5)
    pair_wait(4, po_i, pi_i, pp_ss, pp_rs)
    i_step(1)
    i_pair(2)
    i_pair(6)
    pair_wait(3, po_i, pi_i, pp_ss, pp_rs)
    pair_wait(5, po_i, pi_i, pp_ss, pp_rs)
    i_step(2)
    i_pair(1)
    i_pair(7)
    i_pair(0)
    pair_wait(2, po_i, pi_i, pp_ss, pp_rs)
    pair_wait(6, po_i, pi_i, pp_ss, pp_rs)
    i_step(3)
    pair_wait(1, po_i, pi_i, pp_ss, pp_rs)
    pair_wait(7, po_i, pi_i, pp_ss, pp_rs)
    i_step(4)
    pair_wait(0, po_i, pi_i, pp_ss, pp_rs)
    for h in range(2):
        rows = pl.ds(h * HALF, HALF)
        total = own_i[0, rows, :] + pi_i[0, rows, :].astype(F32)
        for d in range(2):
            i_copy(d, 4, h).wait_recv()
            total = total + irb[d, 3, h].astype(F32)
        own_i[0, rows, :] = total

    f_s[...] = fdot(expd[...], own_i[0].astype(BF16)).reshape(NSP, CAPP, W).astype(BF16)
    j_r[sp] = f_s[sp]

    def j_send(k, _):
        sp_copy(k, f_s, j_r, j_ss, j_rs, True).start()
        return 0

    def j_wait(k, _):
        sp_copy(k, f_s, j_r, j_ss, j_rs, False).wait()
        return 0

    lax.fori_loop(1, NSP, j_send, 0)
    final = hs[...].astype(F32) + scatter_end(own_s, pi_s, sb_s, rb_s, s_ss, s_rs)
    lax.fori_loop(1, NSP, j_wait, 0)
    back = j_r[...].astype(F32).reshape(PROWS, W).astype(BF16)
    for k in range(2):
        pick = onehot(iota((TOK, PROWS), 1) == slot_col(k))
        final = final + fdot(pick, back) * rw[:, k:k + 1]

    j16 = iota((NTP * OWNP, 1), 0)
    spread = onehot(iota((NTP * OWNP, TOK), 1) == jnp.where((j16 & 15) < OWN, OWN * (j16 >> 4) + (j16 & 15), -1))
    l_s[...] = fdot(spread, final.astype(BF16)).astype(BF16).reshape(NTP, OWNP, W)
    l_r[:, lanes(t, W)] = l_s[t]

    def l_copy(k, to):
        tt = lax.rem(t + k, NTP) if to else lax.rem(t + NTP - k, NTP)
        return rcopy(l_s.at[tt], l_r.at[:, lanes(t if to else tt, W)], l_ss.at[k], l_rs.at[k], tdev(tt))

    def l_send(k, _):
        l_copy(k, True).start()
        return 0

    def l_wait(k, _):
        l_copy(k, False).wait()
        return 0

    lax.fori_loop(1, NTP, l_send, 0)
    for off in range(1, NY):
        e_copy(off).wait_send()
    for off in range(NY):
        e_fwd(off, c).wait_send()
    g_own(c).wait_send()
    for k in range(1, 5):
        for h in range(2):
            for d in range(2):
                if ok_g(d, k, h):
                    g_send(d, k, h).wait_send()
                    g_fwd(d, k, h, c).wait_send()
                if k > 1 or h == d:
                    i_copy(d, k, h).wait_send()
    lax.fori_loop(1, NTP, l_wait, 0)
    out[...] = l_r[...]


def post(heads_a, heads_b, residual, norm_gain, routes, route_weights, weights):
    resid = jnp.pad(residual, ((0, OWNP - OWN), (0, 0)))
    dma = pltpu.SemaphoreType.DMA
    vm = pltpu.VMEM
    scratch = [
        vm((64, D), BF16), vm((128, D), BF16), vm((D, 2 * W), BF16), vm((W, D), BF16), vm((D, 2 * W), BF16), vm((W, D), BF16),
        vm((NTP, OWNP, W), BF16), vm((NY, TOK, W), F32), vm((NY, TOK, W), BF16), vm((NY, TOK, W), BF16), vm((NY, TOK, W), BF16), vm((NY, TOK, W), BF16),
        vm((TOK, W), BF16), vm((TOK, D), BF16), vm((TOK, D), BF16),
        vm((NY, TOK, W), BF16), vm((NY, TOK, W), BF16), vm((NY, TOK, W), BF16), vm((NY, TOK, W), BF16), vm((NY, TOK, W), F32),
        vm((NSP, CAPP, W), BF16), vm((NSP, CAPP, W), BF16), vm((ROWS, PROWS), BF16), vm((PROWS, ROWS), BF16), vm((NY, ROWS, 2 * W), BF16), vm((ROWS, 2 * W), F32),
        vm((NY, ROWS, W), F32), vm((NY, ROWS, W), BF16), vm((NY, ROWS, W), BF16), vm((2, 4, 2, HALF, W), BF16), vm((2, 4, 2, HALF, W), BF16),
        vm((NSP, CAPP, W), BF16), vm((NTP, OWNP, W), BF16), vm((OWNP, D), BF16),
        dma((8,)), dma((NTP,)), dma((NTP,)), dma((NY,)), dma((NY,)), dma((NY,)), dma((NY,)), dma((NY,)), dma((NY,)), dma((NY,)), dma((NY,)),
        dma((NY,)), dma((NY,)), dma((NY,)), dma((NY,)), dma((NSP,)), dma((NSP,)),
        dma((2, 4, 2)), dma((2, 4, 2)), dma((2, 4, 2)), dma((2, 4, 2)), dma, dma,
        dma((NY,)), dma((NY,)), dma((2, 4, 2)), dma((2, 4, 2)), dma((NSP,)), dma((NSP,)), dma((NTP,)), dma((NTP,)),
    ]
    vspec = pl.BlockSpec(memory_space=pltpu.VMEM)
    hspec = pl.BlockSpec(memory_space=pl.ANY)
    padded = pl.pallas_call(
        post_kernel,
        out_shape=jax.ShapeDtypeStruct((OWNP, D), BF16),
        in_specs=[vspec] * 7 + [hspec] * 8,
        out_specs=vspec,
        scratch_shapes=scratch,
        compiler_params=pltpu.CompilerParams(collective_id=1, has_side_effects=True, vmem_limit_bytes=60 * 2**20),
        name="post",
    )(heads_a, heads_b, resid, norm_gain.reshape(1, D), routes, routes.T, route_weights, *weights)
    return padded[:OWN]


def sent_together(arrays, axis, dim, along):
    ends, at = ([], 0)
    for a in arrays[:-1]:
        at += a.shape[along]
        ends.append(at)
    both = jnp.concatenate(arrays, axis=along)
    return tuple(jnp.split(lax.all_gather(both, axis, axis=dim, tiled=True), ends, axis=along))


def tables(positions, width):
    half = width // 2
    freqs = theta_base ** (-(2.0 * jnp.arange(half, dtype=jnp.float32)) / width)
    angles = positions.astype(jnp.float32)[:, None] * freqs[None, :]
    return (jnp.cos(angles), jnp.sin(angles))


def rotate(values, cosine, sine):
    half = values.shape[-1] // 2
    first = values[..., :half].astype(jnp.float32)
    second = values[..., half:].astype(jnp.float32)
    turned = jnp.concatenate(
        [first * cosine - second * sine, first * sine + second * cosine], axis=-1
    )
    return turned.astype(jnp.bfloat16)


def group_update(state, queries_nope, queries_rope, keys, values, rot_piece, mask, scale):
    top, total, weighted = state
    scores = jnp.einsum("qhd,khd->hqk", queries_nope, keys, preferred_element_type=jnp.float32)
    scores = scores + jnp.einsum(
        "qhr,kr->hqk", queries_rope, rot_piece, preferred_element_type=jnp.float32
    )
    scores = jnp.where(mask[None], scores * scale, very_low)
    new_top = jnp.maximum(top, jnp.max(scores, axis=-1))
    expo = jnp.where(mask[None], jnp.exp(scores - new_top[..., None]), 0.0)
    total = jnp.sum(expo, axis=-1)
    weighted = jnp.einsum(
        "hqk,khv->hqv", expo.astype(jnp.bfloat16), values, preferred_element_type=jnp.float32
    )
    return (new_top, total, weighted)


def empty_state(heads, rows, vsize):
    return (
        jnp.full((heads, rows), very_low, jnp.float32),
        jnp.zeros((heads, rows), jnp.float32),
        jnp.zeros((heads, rows, vsize), jnp.float32),
    )


def shards(
    residual,
    query_a,
    query_b,
    latents,
    rope_key,
    key_up_a,
    value_up_a,
    key_up_b,
    value_up_b,
    out_proj_a,
    out_proj_b,
    norm_gain,
    routes,
    route_weights,
    shared_gate,
    shared_up,
    shared_down,
    expert_gate,
    expert_up,
    expert_down,
):
    tok = query_a.shape[0]
    heads_a = key_up_a.shape[1] // DA
    heads_b = key_up_b.shape[1] // DB
    first_row = lax.axis_index(SP) * tok
    last_row = first_row + tok
    query_pos = first_row + jnp.arange(tok, dtype=jnp.int32)
    cosine, sine = tables(query_pos, ROPE)
    rot_key = rotate(rope_key, cosine, sine)
    shaped_a = query_a.reshape(tok, heads_a, DA + ROPE)
    shaped_b = query_b.reshape(tok, heads_b, DB + ROPE)
    nope_a = shaped_a[..., :DA]
    nope_b = shaped_b[..., :DB]
    turned_a = rotate(shaped_a[..., DA:], cosine[:, None, :], sine[:, None, :])
    turned_b = rotate(shaped_b[..., DB:], cosine[:, None, :], sine[:, None, :])
    scale_a = (DA + ROPE) ** (-0.5)
    scale_b = (DB + ROPE) ** (-0.5)

    def attend(state, keys_a, values_a, keys_b, values_b, rot_piece, key_pos):
        count = keys_a.shape[0]
        mask = key_pos[None, :] <= query_pos[:, None]
        state_a = group_update(
            state[0],
            nope_a,
            turned_a,
            keys_a.reshape(count, heads_a, DA),
            values_a.reshape(count, heads_a, VA),
            rot_piece,
            mask,
            scale_a,
        )
        state_b = group_update(
            state[1],
            nope_b,
            turned_b,
            keys_b.reshape(count, heads_b, DB),
            values_b.reshape(count, heads_b, VB),
            rot_piece,
            mask,
            scale_b,
        )
        return (state_a, state_b)

    start_state = (empty_state(heads_a, tok, VA), empty_state(heads_b, tok, VB))
    keys_a = jnp.dot(latents, key_up_a, preferred_element_type=jnp.float32).astype(jnp.bfloat16)
    values_a = jnp.dot(latents, value_up_a, preferred_element_type=jnp.float32).astype(jnp.bfloat16)
    keys_b = jnp.dot(latents, key_up_b, preferred_element_type=jnp.float32).astype(jnp.bfloat16)
    values_b = jnp.dot(latents, value_up_b, preferred_element_type=jnp.float32).astype(jnp.bfloat16)
    keys_a, values_a, keys_b, values_b = (keys_a, values_a, keys_b, values_b)
    piece = sent_together((keys_a, values_a, keys_b, values_b, rot_key), SP, 0, 1)
    key_pos = jnp.arange(piece[0].shape[0], dtype=jnp.int32)

    def compute(inner):
        return attend(inner, piece[0], piece[1], piece[2], piece[3], piece[4], key_pos)

    state = lax.cond(jnp.int32(0) < last_row, compute, lambda inner: inner, start_state)
    heads_out_a = (state[0][2] / state[0][1][..., None]).astype(jnp.bfloat16)
    heads_out_b = (state[1][2] / state[1][1][..., None]).astype(jnp.bfloat16)
    heads_out_a = heads_out_a.transpose(1, 0, 2).reshape(tok, heads_a * VA)
    heads_out_b = heads_out_b.transpose(1, 0, 2).reshape(tok, heads_b * VB)
    weights = (
        out_proj_a, out_proj_b, shared_gate, shared_up, shared_down,
        expert_gate[0], expert_up[0], expert_down[0],
    )
    return post(heads_out_a, heads_out_b, residual, norm_gain, routes, route_weights, weights)


def solution(mesh):
    torus = Mesh(mesh.devices.reshape(NZ, NX, NY, NC), ALL)
    in_specs = (
        P(SP + TP, None),
        P(SP, TP),
        P(SP, TP),
        P(SP, None),
        P(SP, None),
        P(None, TP),
        P(None, TP),
        P(None, TP),
        P(None, TP),
        P(TP, None),
        P(TP, None),
        P(),
        P(SP, None),
        P(SP, None),
        P(None, TP),
        P(None, TP),
        P(TP, None),
        P(SP, None, TP),
        P(SP, None, TP),
        P(SP, TP, None),
    )
    return jax.shard_map(
        shards, mesh=torus, in_specs=in_specs, out_specs=P(SP + TP, None), check_vma=False
    )
```

time: 426 us -> 247 us (0.58)
  blocking collectives: 134 us -> 0 us
  Pallas kernels: 0 us -> 105 us
  waiting for transfers between devices: 188 us -> 93 us
  local copies, waits for them, and re-layouts: 27.9 us -> 10.2 us
  starting transfers between devices: 15.4 us -> 0.01 us
  matrix products: 32 us -> 19.8 us
  other arithmetic: 14 us -> 5.3 us
    all_to_all x2 -> x0, blocking collectives: 112 us -> none  [the longest x1 71.6 us: shards(): lax.all_to_all(outgoing, 'sp', split_axis=0, concat_axis=0, tiled=True)]
    pallas_call x0 -> x1, Pallas kernels: none -> 105 us  [post(): pl.pallas_call(post_kernel, out_shape=jax.ShapeDtypeStruct((OWNP, D), BF1...]
    all_to_all x2 -> x0, waiting for transfers between devices: 90.4 us -> none  [the longest x1 64.5 us: shards(): lax.all_to_all(part.reshape(sources, items, down_w.shape[1]), 'sp', split...]
    all_gather x2 -> x0, blocking collectives: 22.5 us -> none  [whole_of(): value = lax.all_gather(value, axis, axis=dim, tiled=True)]
    all_to_all x2 -> x0, starting transfers between devices: 15.4 us -> none  [the longest x1 7.95 us: sum_at_owner(): lax.all_to_all(tiles, axis, split_axis=0, concat_axis=0, tiled=True)]
    reshape x6 -> x0, local copies, waits for them, and re-layouts: 15.1 us -> none  [the longest x1 4.4 us: shards(): part.reshape(sources, items, down_w.shape[1])]
    dot_general x7 -> x0, matrix products: 11.6 us -> none  [the longest x1 5.04 us: shards(): jnp.dot(act, down_w, preferred_element_type=jnp.float32)]
    reduce_sum x6 -> x0, other arithmetic: 8.35 us -> none  [the longest x1 7.59 us: shards(): jnp.sum(picked * route_weights[..., None], axis=1)]
  transfers between devices with their start and end apart: 3 -> 1, of which waited for: 3 -> 1; matrix products, arithmetic and copies ran while one was open for 1% -> 3% of each run, Pallas kernels for 0% -> 0%
where the time goes in v1:
time: 247 us
  Pallas kernels  105 us (43%)
  waiting for transfers between devices  93 us (38%)
  matrix products  19.8 us (8%)
  between operations  13.5 us (5%)
  local copies, waits for them, and re-layouts  10.2 us (4%)
  other arithmetic  5.3 us (2%)
    pallas_call x1, Pallas kernels, post(): pl.pallas_call(post_kernel, out_shape=jax.ShapeDtypeStruct((OWNP, D), BF1...  105 us
    all_gather x1, waiting for transfers between devices, sent_together(): lax.all_gather(both, axis, axis=dim, tiled=True)  93 us
    dot_general x2, matrix products, group_update(): jnp.einsum('qhr,kr->hqk', queries_rope, rot_piece, preferred_element_type...  8.34 us
    unnamed x7, local copies, waits for them, and re-layouts  5.41 us
  transfers between devices with their start and end apart: 1, of which 1 were waited for; matrix products, arithmetic and copies ran while one was open for 3% of the time, Pallas kernels for 0%

profile of v1, /device:TPU:1, one launch (start us, length us, event | category | flops | bytes accessed | tf_op | source)
XLA Modules:
  0.0 246.6 jit_solution(3413493234351759259)
XLA Ops:
  6.6 0.9 copy-done
  7.5 1.0 convolution_convert_fusion.3
  8.6 1.0 convolution_convert_fusion.2
  9.7 1.1 convolution_convert_fusion.1
  10.9 1.1 convolution_convert_fusion
  12.0 0.9 fusion.51
  13.1 0.8 concatenate.30
  13.9 1.0 fusion.62
  15.0 1.5 copy.66.routes
  16.5 1.4 copy.67.rw
  17.9 1.5 pad.4.resid
  19.4 0.9 fusion.57
  20.3 93.0 %all-gather.2.cloned.1.call-done = bf16[6144,416]{1,0:T(8,128)(2,1)} async-done(((bf16[192,416]{1,0:T(8,128)(2,1)}), bf16[6144,416]{1,0:T(8,128)(2,1)}) %all-gather.2.cloned.1.call-update) | async-done | bytes 5111824 | tf_op jit(solution)/shard_map/all_gather | solution.py:462
  113.3 18.9 %conditional.1 = (f32[1,192]{1,0:T(1,128)S(1)}, f32[1,192]{1,0:T(1,128)S(1)}, f32[1,192,128]{2,1,0:T(8,128)S(1)}, f32[1,192,64]{2,1,0:T(8,128)S(1)}) conditional(s32[]{:T(128)} %convert_element_type.73, () %tuple.13, (s32[6144]{0:T(1024)S(1)}, s32[]{:T(128)}, s32[192]{0:T(256)S(1)}, bf16[192,1,96]{2,0,1:T(8,128)(2,1)}, bf16[6144,416]{1,0:T(8,128)(2,1)}, ...), branch_computations={%region_0.0_spmd, %region_1.6_spmd} | conditional | flops 1086455552 | bytes 90389920 | solution.py:582
  113.3 1.0 copy.64
  114.3 2.2 convolution_bitcast_fusion.1
  116.5 5.0 %fusion.60 = (f32[192]{0:T(256)S(1)}, f32[1,192,6144]{2,1,0:T(8,128)}) fusion(f32[1,192,6144]{2,1,0:T(8,128)S(1)} %convolution_bitcast_fusion.1, bf16[192,1,32]{0,2,1:T(8,128)(2,1)S(1)} %get-tuple-element.41, bf16[6144,416]{1,0:T(8,128)(2,1)} %get-tuple-element.38, s32[192]{0:T(256)S(1)} %broadcast_add_fusion, s32[6144]{0:T(1024)S(1)} %get-tuple-element.34), kind=kOutput, calls=%fused_computation.77 | convolution fusion | flops 81395520 | bytes 11048448 | tf_op jit(solution)/shard_map/cond/branch_1_fun/qhr,kr->hqk/dot_general | solution.py:485
  121.6 2.4 convolution_bitcast_fusion.3
  124.0 3.4 %fusion.61 = (f32[192]{0:T(256)S(1)}, f32[1,192,6144]{2,1,0:T(8,128)S(1)}) fusion(f32[1,192,6144]{2,1,0:T(8,128)S(1)} %convolution_bitcast_fusion.3, bf16[192,1,32]{0,2,1:T(8,128)(2,1)S(1)} %get-tuple-element.39, bf16[6144,416]{1,0:T(8,128)(2,1)} %get-tuple-element.38, s32[192]{0:T(256)S(1)} %broadcast_add_fusion, s32[6144]{0:T(1024)S(1)} %get-tuple-element.34), kind=kOutput, calls=%fused_computation.78 | convolution fusion | flops 81395520 | bytes 11048448 | tf_op jit(solution)/shard_map/cond/branch_1_fun/qhr,kr->hqk/dot_general | solution.py:485
  127.4 2.1 fusion.7
  129.5 1.2 fusion.20
  130.7 1.5 fusion.25
  133.6 104.6 %post.1 = bf16[16,2048]{1,0:T(8,128)(2,1)} custom-call(bf16[192,64]{1,0:T(8,128)(2,1)} %fusion.34.heads_a, bf16[192,128]{1,0:T(8,128)(2,1)} %fusion.35.heads_b, bf16[16,2048]{1,0:T(8,128)(2,1)} %pad.4.resid, f32[1,2048]{1,0:T(1,128)} %bitcast.91, s32[192,2]{1,0:T(8,128)} %copy.66.routes, s32[2,192]{1,0:T(2,128)} %bitcast.92, f32[192,2]{1,0:T(8,128)} %copy.67.rw, ...), custom_call_target="tpu_custom_call" | custom-call | tf_op jit(solution)/shard_map/post/pallas_call | solution.py:444
  238.3 1.5 copy.81
  (31 shorter events, 2.2 us)
Async XLA Ops:
  6.5 0.9 copy-start
  6.5 106.7 %all-gather.2.cloned.1.call-start = ((), (), s32[]{:S(2)}) async-start(), calls=%async_computation | async-start | bytes 6488064 | tf_op jit(solution)/shard_map/all_gather | solution.py:462
  116.5 5.0 %copy-start.1 = (bf16[192,1,96]{2,0,1:T(8,128)(2,1)S(1)}, bf16[192,1,96]{2,0,1:T(8,128)(2,1)}, u32[]{:S(2)}) copy-start(bf16[192,1,96]{2,0,1:T(8,128)(2,1)} %get-tuple-element.69) | copy-start | bytes 110596 | tf_op jit(solution)/shard_map/cond
  121.6 5.8 %slice-start = ((s8[4718592]{0:T(1024)(128)(4,1)}), s8[4194304]{0:T(1024)(128)(4,1)S(1)}, s32[]{:S(2)}) async-start(s8[4718592]{0:T(1024)(128)(4,1)} %bitcast.79), calls=%async_computation.1 | async-start | bytes 8388608 | tf_op jit(solution)/shard_map/cond
  121.6 7.9 %slice-start.2 = ((s8[6291456]{0:T(1024)(128)(4,1)}), s8[4194304]{0:T(1024)(128)(4,1)S(1)}, s32[]{:S(2)}) async-start(s8[6291456]{0:T(1024)(128)(4,1)} %bitcast.81), calls=%async_computation.3 | async-start | bytes 8388608 | tf_op jit(solution)/shard_map/cond
  124.0 3.4 %slice-start.1 = ((s8[4718592]{0:T(1024)(128)(4,1)}), s8[524288]{0:T(1024)(128)(4,1)S(1)}, s32[]{:S(2)}) async-start(s8[4718592]{0:T(1024)(128)(4,1)} %bitcast.79), calls=%async_computation.2 | async-start | bytes 1048576 | tf_op jit(solution)/shard_map/cond
  124.0 5.5 %slice-start.3 = ((s8[6291456]{0:T(1024)(128)(4,1)}), s8[2097152]{0:T(1024)(128)(4,1)S(1)}, s32[]{:S(2)}) async-start(s8[6291456]{0:T(1024)(128)(4,1)} %bitcast.81), calls=%async_computation.4 | async-start | bytes 4194304 | tf_op jit(solution)/shard_map/cond
Sparse Core Ops, SparseCore 0:
  14.0 99.2 all-gather.1

commit v2 on v1

v2 whole, which is shorter than its diff:
```python
import functools

import jax
import jax.numpy as jnp
from jax import lax
from jax.experimental import pallas as pl
from jax.experimental.pallas import tpu as pltpu
from jax.sharding import Mesh
from jax.sharding import PartitionSpec as P

DA = 64
VA = 64
DB = 128
VB = 128
ROPE = 32
TOK = 192
D = 2048
W = 128
CAP = 18
CAPP = 24
NZ, NX, NY, NC = 4 * 2, 4, 8, 2
NSP = NZ * NX
NTP = NY * NC
ROWS = NSP * CAP
PROWS = NSP * CAPP
HALF = ROWS // 2
OWN = TOK // NTP
OWNP = 16
SP = ("z", "x")
TP = ("y", "c")
ALL = ("z", "x", "y", "c")
MESH_ID = pl.DeviceIdType.MESH
F32 = jnp.float32
BF16 = jnp.bfloat16
FAR_FIRST = (4, 3, 5, 2, 6, 1, 7, 0)

theta_base = 10000.0
norm_eps = 1e-06
very_low = -1e30
RATE_A = 1.4426950408889634 * (DA + ROPE) ** (-0.5)
RATE_B = 1.4426950408889634 * (DB + ROPE) ** (-0.5)


def fdot(a, b):
    return jnp.dot(a, b, preferred_element_type=F32)


def rcopy(src, dst, ssem, rsem, dev):
    return pltpu.make_async_remote_copy(
        src_ref=src, dst_ref=dst, send_sem=ssem, recv_sem=rsem, device_id=dev, device_id_type=MESH_ID
    )


def iota(shape, dim):
    return lax.broadcasted_iota(jnp.int32, shape, dim)


def onehot(cond):
    return jnp.where(cond, 1.0, 0.0).astype(BF16)


def lanes(index, width):
    return pl.ds(pl.multiple_of(index * width, 128), width)


def nt(a, b):
    return lax.dot_general(a, b, (((1,), (1,)), ((), ())), preferred_element_type=F32)


def layer_kernel(
    qa, qb, lat, rope, cosine, sine, kua, kub, vua, vub,
    resid, gain, routes_t, rw_t,
    oa_h, ob_h, sg_h, su_h, sd_h, eg_h, eu_h, ed_h,
    out,
    lz, q_all, wv_t, m_a, l_a, m_b, l_b, acc_a, acc_b, ps, st, pr, sr, heads, cols8,
    wo, sgu, sd, egu, ed,
    r_s, r_r, own_d, po_d, pi_d, sb_d, rb_d,
    hs, hfull, normed,
    po_s, pi_s, sb_s, rb_s, own_s,
    f_s, f_r, comp, expd, g, hacc,
    own_i, po_i, pi_i, isb, irb, j_r, l_s, l_r,
    z_ss, z_rs, zf_ss, zf_rs, zo_ss, zo_rs, q_ss, q_rs, x_ss, x_rs, t_ss, t_rs,
    w_sem, r_ss, r_rs, pd_ss, pd_rs, d_ss, d_rs, e_ss, e_rs, ef_ss, ef_rs,
    ps_ss, ps_rs, s_ss, s_rs, f_ss, f_rs, g_ss, g_rs, gf_ss, gf_rs, go_ss, go_rs,
    pp_ss, pp_rs, i_ss, i_rs, j_ss, j_rs, l_ss, l_rs,
):
    z, x, y, c = (lax.axis_index(a) for a in ALL)
    t = y * NC + c
    sp = z * NX + x
    oc = 1 - c
    partner = (z, x, y, oc)

    def ydev(yy):
        return (z, x, yy, c)

    def tdev(tt):
        return (z, x, tt // NC, lax.rem(tt, NC))

    def sdev(ss):
        return (ss // NX, lax.rem(ss, NX), y, c)

    def xdev(xx):
        return (z, xx, y, c)

    def zdev(zz):
        return (zz, x, y, c)

    def yoff(off):
        return lax.rem(y + off, NY)

    class Ring:
        def __init__(self, pos, dev, win, sems):
            self.pos, self.dev, self.win = pos, dev, win
            self.ss, self.rs, self.fs, self.fr, self.os, self.orr = sems

        def src(self, d, k):
            return lax.rem(self.pos + 8 - k, 8) if d == 0 else lax.rem(self.pos + k, 8)

        def to(self, d):
            return self.dev(self.src(1 - d, 1))

        def ok(self, k, d, h):
            return k < 4 or h == d

        def send(self, d, k, h):
            win = self.win(self.src(d, k - 1), h, c)
            return rcopy(win, win, self.ss.at[d, k - 1, h], self.rs.at[d, k - 1, h], self.to(d))

        def got(self, d, k, h):
            win = self.win(self.src(d, k), h, c)
            return rcopy(win, win, self.ss.at[d, k - 1, h], self.rs.at[d, k - 1, h], self.to(d))

        def fwd(self, d, k, h, core):
            win = self.win(self.src(d, k), h, core)
            return rcopy(win, win, self.fs.at[d, k - 1, h], self.fr.at[d, k - 1, h], partner)

        def own(self, h, core):
            win = self.win(self.pos, h, core)
            return rcopy(win, win, self.os.at[h], self.orr.at[h], partner)

        def run(self, use, own_too, before_use):
            for h in range(2):
                for d in range(2):
                    self.send(d, 1, h).start()
                if own_too:
                    self.own(h, c).start()
            for k in range(1, 5):
                for h in range(2):
                    for d in range(2):
                        if self.ok(k, d, h):
                            self.got(d, k, h).wait_recv()
                            if self.ok(k + 1, d, h) and k < 4:
                                self.send(d, k + 1, h).start()
                            self.fwd(d, k, h, c).start()
                if k == 1:
                    before_use()
                    if own_too:
                        for h in range(2):
                            self.own(h, oc).wait_recv()
                    use(self.pos, True)
                else:
                    for d in range(2):
                        for h in range(2):
                            self.fwd(d, k - 1, h, oc).wait_recv()
                        use(self.src(d, k - 1), False)
            self.fwd(0, 4, 0, oc).wait_recv()
            self.fwd(1, 4, 1, oc).wait_recv()
            use(self.src(0, 4), False)

        def finish(self, own_too):
            for h in range(2):
                if own_too:
                    self.own(h, c).wait_send()
                for k in range(1, 5):
                    for d in range(2):
                        if self.ok(k, d, h):
                            self.send(d, k, h).wait_send()
                            self.fwd(d, k, h, c).wait_send()

    weights = [
        (ob_h, wo.at[0:VB]), (oa_h, wo.at[VB:VB + VA]), (sg_h, sgu.at[:, 0:W]), (su_h, sgu.at[:, W:2 * W]), (sd_h, sd),
        (eg_h, egu.at[:, 0:W]), (eu_h, egu.at[:, W:2 * W]), (ed_h, ed),
    ]
    loads = [pltpu.make_async_copy(a, b, w_sem.at[i]) for i, (a, b) in enumerate(weights)]
    for load in loads:
        load.start()

    barrier = pltpu.get_barrier_semaphore()

    def greet_t(k, _):
        pl.semaphore_signal(barrier, inc=1, device_id=tdev(lax.rem(t + k, NTP)), device_id_type=MESH_ID)
        return 0

    def greet_s(k, _):
        pl.semaphore_signal(barrier, inc=1, device_id=sdev(lax.rem(sp + k, NSP)), device_id_type=MESH_ID)
        return 0

    lax.fori_loop(1, NTP, greet_t, 0)
    lax.fori_loop(1, NSP, greet_s, 0)

    def turn(value):
        wide = value.astype(F32)
        swapped = jnp.concatenate([wide[:, ROPE // 2:], wide[:, 0:ROPE // 2]], axis=1)
        return wide * cosine[...] + swapped * sine[...]

    rot = turn(rope[...])
    lz[z, :, 0:512] = lat[...]
    lz[z, :, 512:640] = jnp.concatenate([jnp.zeros((TOK, 64), F32), rot, rot], axis=1).astype(BF16)
    wide_a, wide_b = qa[...], qb[...]
    q_all[x] = jnp.concatenate(
        [
            wide_b[:, 0:DB].astype(F32),
            wide_a[:, 0:DA].astype(F32),
            turn(wide_a[:, DA:DA + ROPE]),
            turn(wide_b[:, DB:DB + ROPE]),
        ],
        axis=1,
    ).astype(BF16)
    wv_t[0:VB] = nt(onehot(iota((VB, VB), 0) == iota((VB, VB), 1)), vub[...]).astype(BF16)
    wv_t[VB:VB + VA] = nt(onehot(iota((VA, VA), 0) == iota((VA, VA), 1)), vua[...]).astype(BF16)

    names_t = onehot((iota((128, TOK), 0) == routes_t[0:1, :]) | (iota((128, TOK), 0) == routes_t[1:2, :]))
    upper = onehot(iota((TOK, TOK), 0) < iota((TOK, TOK), 1))
    before_t = fdot(names_t, upper)

    def slot_row(k):
        rank = jnp.sum(jnp.where(iota((128, TOK), 0) == routes_t[k:k + 1, :], before_t, 0.0), axis=0, keepdims=True)
        return routes_t[k:k + 1, :] * CAPP + rank.astype(jnp.int32)

    r_s[...] = jnp.zeros_like(r_s)
    r_s[0:OWN, :] = resid[...]

    i_col = iota((ROWS, 1), 0)
    comp[...] = onehot(iota((ROWS, PROWS), 1) == i_col + (CAPP - CAP) * ((i_col * 3641) >> 16))
    j_col = iota((PROWS, 1), 0)
    j_q = (j_col * 2731) >> 16
    j_r0 = j_col - CAPP * j_q
    expd[...] = onehot(iota((PROWS, ROWS), 1) == jnp.where(j_r0 < CAP, CAP * j_q + j_r0, -1))

    pl.semaphore_wait(barrier, NTP - 1 + NSP - 1)

    def resid_copy(k, to):
        tt = lax.rem(t + k, NTP) if to else lax.rem(t + NTP - k, NTP)
        return rcopy(r_s.at[:, lanes(tt if to else t, W)], r_r.at[t if to else tt], r_ss.at[k], r_rs.at[k], tdev(tt))

    def resid_send(k, _):
        resid_copy(k, True).start()
        return 0

    r_r[t] = r_s[:, lanes(t, W)]

    def pair_out(value, off, own, po, pi, ss, rs):
        left, right = value[:, 0:W], value[:, W:2 * W]
        own[off] = jnp.where(c == 0, left, right)
        po[off] = jnp.where(c == 0, right, left).astype(BF16)
        rcopy(po.at[off], pi.at[off], ss.at[off], rs.at[off], partner).start()

    def pair_wait(off, po, pi, ss, rs):
        rcopy(po.at[off], pi.at[off], ss.at[off], rs.at[off], partner).wait()

    def y_copy(off, sb, rb, ss, rs):
        return rcopy(sb.at[off], rb.at[off], ss.at[off], rs.at[off], ydev(yoff(off)))

    def scatter_start(cols, own, po, pi, sb, rb, pss, prs, ss, rs, lead=3):
        for n in range(NY + lead):
            if n < NY:
                off = FAR_FIRST[n]
                pair_out(cols(yoff(off)), off, own, po, pi, pss, prs)
            if n >= lead:
                off = FAR_FIRST[n - lead]
                pair_wait(off, po, pi, pss, prs)
                if off:
                    sb[off] = (own[off] + pi[off].astype(F32)).astype(BF16)
                    y_copy(off, sb, rb, ss, rs).start()

    def scatter_end(own, pi, sb, rb, ss, rs):
        total = own[0] + pi[0].astype(F32)
        for off in range(1, NY):
            y_copy(off, sb, rb, ss, rs).wait()
            total = total + rb[off].astype(F32)
        return total

    def z_win(zz, h, core):
        start = pl.multiple_of(core * (TOK // 2) + h * (TOK // 4), TOK // 4)
        return lz.at[zz, pl.ds(start, TOK // 4), :]

    def q_copy(off, to):
        src = x if to else lax.rem(x + NX - off, NX)
        return rcopy(q_all.at[src], q_all.at[src], q_ss.at[off], q_rs.at[off], xdev(lax.rem(x + off, NX)))

    def queries_here():
        lax.fori_loop(1, NTP, resid_send, 0)
        for off in (2, 1, 3):
            q_copy(off, False).wait_recv()

    def block(zz, first):
        rows = lz[zz]
        part, twice = rows[:, 0:512], rows[:, 512:640].astype(F32)
        lane = iota((TOK, 128), 1)
        keys_b = fdot(part, kub[...])
        keys_a = jnp.concatenate([fdot(part, kua[...]), twice[:, 64:128]], axis=1)
        keys_a = jnp.where(lane < 96, keys_a, 0.0).astype(BF16)
        keys_b = jnp.concatenate([keys_b, jnp.where(lane < 96, 0.0, twice)], axis=1).astype(BF16)
        values = nt(wv_t[...], part).astype(BF16)
        queries = q_all[...].reshape(NX * TOK, 256)
        if first:
            shape = (TOK, NX * TOK)
            seen = x * TOK + iota(shape, 0) <= iota(shape, 1)
        for scores, rate, m, l, acc, lo, hi in (
            (nt(keys_b, queries), RATE_B, m_b, l_b, acc_b, 0, VB),
            (nt(keys_a, queries[:, 128:256]), RATE_A, m_a, l_a, acc_a, VB, VB + VA),
        ):
            if first:
                scores = jnp.where(seen, scores, very_low)
                top = jnp.max(scores, axis=0, keepdims=True)
                expo = jnp.where(seen, jnp.exp2((scores - top) * rate), 0.0)
                l[...] = jnp.sum(expo, axis=0, keepdims=True)
                acc[...] = fdot(values[lo:hi], expo.astype(BF16))
            else:
                top = jnp.maximum(m[...], jnp.max(scores, axis=0, keepdims=True))
                expo = jnp.exp2((scores - top) * rate)
                fade = jnp.exp2((m[...] - top) * rate)
                l[...] = l[...] * fade + jnp.sum(expo, axis=0, keepdims=True)
                acc[...] = acc[...] * fade + fdot(values[lo:hi], expo.astype(BF16))
            m[...] = top

    def use_block(zz, first):
        if first:
            block(zz, True)
        else:
            pl.when(zz < z)(lambda: block(zz, False))

    z_ring = Ring(z, zdev, z_win, (z_ss, z_rs, zf_ss, zf_rs, zo_ss, zo_rs))
    for off in (2, 1, 3):
        q_copy(off, True).start()
    z_ring.run(use_block, False, queries_here)

    share_b = jnp.where(l_b[...] > 0, 1.0 / l_b[...], 0.0)
    share_a = jnp.where(l_a[...] > 0, 1.0 / l_a[...], 0.0)
    out_b, out_a = (acc_b[...] * share_b).astype(BF16), (acc_a[...] * share_a).astype(BF16)
    for xx in range(NX):
        cut = slice(xx * TOK, (xx + 1) * TOK)
        ps[xx, 0:VB] = out_b[:, cut]
        ps[xx, VB:VB + VA] = out_a[:, cut]
        for i, stat in enumerate((m_b, l_b, m_a, l_a)):
            st[xx, i:i + 1, :] = stat[:, cut]
            st[xx, i + 4:i + 5, :] = stat[:, cut]

    def x_copy(src, dst, ss, rs, off, to):
        there = lax.rem(x + off, NX) if to else lax.rem(x + NX - off, NX)
        return rcopy(src.at[there], dst.at[x if to else there], ss.at[off], rs.at[off], xdev(there))

    for off in (2, 1, 3):
        x_copy(st, sr, t_ss, t_rs, off, True).start()
        x_copy(ps, pr, x_ss, x_rs, off, True).start()
    pr[x] = ps[x]
    sr[x] = st[x]
    for load in loads[:2]:
        load.wait()
    for off in range(1, NX):
        x_copy(st, sr, t_ss, t_rs, off, False).wait()
        x_copy(ps, pr, x_ss, x_rs, off, False).wait()
    merged = []
    for row, rate, lo, hi in ((0, RATE_B, 0, VB), (2, RATE_A, VB, VB + VA)):
        tops = [sr[i, row:row + 1, :] for i in range(NX)]
        top = functools.reduce(jnp.maximum, tops)
        part = [jnp.exp2((tops[i] - top) * rate) * sr[i, row + 1:row + 2, :] for i in range(NX)]
        whole = 1.0 / sum(part)
        merged.append(sum(pr[i, lo:hi].astype(F32) * (part[i] * whole) for i in range(NX)))
    turned = jnp.concatenate(merged, axis=0).astype(BF16)
    heads[...] = nt(onehot(iota((TOK, TOK), 0) == iota((TOK, TOK), 1)), turned).astype(BF16)

    def head_cols(yy):
        return fdot(heads[...], wo[:, lanes(yy, 2 * W)])

    scatter_start(head_cols, own_d, po_d, pi_d, sb_d, rb_d, pd_ss, pd_rs, d_ss, d_rs)

    def resid_wait(k, _):
        resid_copy(k, False).wait()
        return 0

    mixed = scatter_end(own_d, pi_d, sb_d, rb_d, d_ss, d_rs)
    lax.fori_loop(1, NTP, resid_wait, 0)
    i12 = iota((TOK, 1), 0)
    pick12 = onehot(iota((TOK, NTP * OWNP), 1) == i12 + (OWNP - OWN) * ((i12 * 5462) >> 16))
    resid_cols = fdot(pick12, r_r[...].reshape(NTP * OWNP, W))
    hs[...] = (resid_cols + mixed).astype(BF16)

    hfull[:, lanes(t, W)] = hs[...]

    def e_copy(off):
        return rcopy(hs, hfull.at[:, lanes(t, W)], e_ss.at[off], e_rs.at[off], ydev(yoff(off)))

    def e_got(off):
        src = lanes(lax.rem(y + NY - off, NY) * NC + c, W)
        return rcopy(hs, hfull.at[:, src], e_ss.at[off], e_rs.at[off], ydev(yoff(off)))

    def e_fwd(off, core):
        win = hfull.at[:, lanes(lax.rem(y + NY - off, NY) * NC + core, W)]
        return rcopy(win, win, ef_ss.at[off], ef_rs.at[off], partner)

    for off in FAR_FIRST[:-1]:
        e_copy(off).start()
    e_fwd(0, c).start()
    for off in (1, 7, 2, 6, 3, 5, 4):
        e_got(off).wait_recv()
        e_fwd(off, c).start()
    for off in range(NY):
        e_fwd(off, oc).wait_recv()

    def norm_rows(b, _):
        rows = pl.ds(pl.multiple_of(b * 16, 16), 16)
        wide = hfull[rows, :].astype(F32)
        mean = jnp.mean(wide * wide, axis=-1, keepdims=True)
        normed[rows, :] = (wide * lax.rsqrt(mean + norm_eps) * gain[...]).astype(BF16)
        return 0

    lax.fori_loop(0, TOK // 16, norm_rows, 0)

    place = onehot((iota((PROWS, TOK), 0) == slot_row(0)) | (iota((PROWS, TOK), 0) == slot_row(1)))
    f_s[...] = fdot(place, normed[:, lanes(t, W)]).reshape(NSP, CAPP, W).astype(BF16)
    f_r[sp] = f_s[sp]

    def sp_copy(k, src, dst, ss, rs, to):
        peer = lax.rem(sp + k, NSP) if to else lax.rem(sp + NSP - k, NSP)
        return rcopy(src.at[peer], dst.at[sp if to else peer], ss.at[k], rs.at[k], sdev(peer))

    def f_send(k, _):
        sp_copy(k, f_s, f_r, f_ss, f_rs, True).start()
        return 0

    def f_wait(k, _):
        sp_copy(k, f_s, f_r, f_ss, f_rs, False).wait()
        return 0

    lax.fori_loop(1, NSP, f_send, 0)

    for load in loads[2:]:
        load.wait()
    both = fdot(normed[...], sgu[...])
    gate, up = both[:, 0:W], both[:, W:2 * W]
    shared_act = (gate / (1.0 + jnp.exp(-gate)) * up).astype(BF16)

    def shared_cols(yy):
        return fdot(shared_act, sd[:, lanes(yy, 2 * W)])

    scatter_start(shared_cols, own_s, po_s, pi_s, sb_s, rb_s, ps_ss, ps_rs, s_ss, s_rs)

    lax.fori_loop(1, NSP, f_wait, 0)
    g[y, :, lanes(c, W)] = fdot(comp[...], f_r[...].astype(F32).reshape(PROWS, W).astype(BF16)).astype(BF16)

    def g_win(yy, h, core):
        return g.at[yy, pl.ds(h * HALF, HALF), lanes(core, W)]

    def gate_up(yy, first):
        value = fdot(g[yy], egu[pl.ds(pl.multiple_of(yy * 2 * W, 2 * W), 2 * W), :])
        hacc[...] = value if first else hacc[...] + value

    y_ring = Ring(y, ydev, g_win, (g_ss, g_rs, gf_ss, gf_rs, go_ss, go_rs))
    y_ring.run(gate_up, True, lambda: None)
    gate, up = hacc[:, 0:W], hacc[:, W:2 * W]
    act = (gate / (1.0 + jnp.exp(-gate)) * up).astype(BF16)

    def i_pair(off):
        pair_out(fdot(act, ed[:, lanes(yoff(off), 2 * W)]), off, own_i, po_i, pi_i, pp_ss, pp_rs)

    def i_copy(d, k, h):
        return rcopy(isb.at[d, k - 1, h], irb.at[d, k - 1, h], i_ss.at[d, k - 1, h], i_rs.at[d, k - 1, h], y_ring.to(d))

    def i_step(k):
        for h in range(2):
            for d in range(2):
                if k > 1 or h == d:
                    off = (5 - k) if d == 0 else (3 + k)
                    rows = pl.ds(h * HALF, HALF)
                    total = own_i[off, rows, :] + pi_i[off, rows, :].astype(F32)
                    if k > 2 or (k == 2 and h == d):
                        i_copy(d, k - 1, h).wait_recv()
                        total = total + irb[d, k - 2, h].astype(F32)
                    isb[d, k - 1, h] = total.astype(BF16)
                    i_copy(d, k, h).start()

    i_pair(4)
    i_pair(3)
    i_pair(5)
    pair_wait(4, po_i, pi_i, pp_ss, pp_rs)
    i_step(1)
    i_pair(2)
    i_pair(6)
    pair_wait(3, po_i, pi_i, pp_ss, pp_rs)
    pair_wait(5, po_i, pi_i, pp_ss, pp_rs)
    i_step(2)
    i_pair(1)
    i_pair(7)
    i_pair(0)
    pair_wait(2, po_i, pi_i, pp_ss, pp_rs)
    pair_wait(6, po_i, pi_i, pp_ss, pp_rs)
    i_step(3)
    pair_wait(1, po_i, pi_i, pp_ss, pp_rs)
    pair_wait(7, po_i, pi_i, pp_ss, pp_rs)
    i_step(4)
    pair_wait(0, po_i, pi_i, pp_ss, pp_rs)
    for h in range(2):
        rows = pl.ds(h * HALF, HALF)
        total = own_i[0, rows, :] + pi_i[0, rows, :].astype(F32)
        for d in range(2):
            i_copy(d, 4, h).wait_recv()
            total = total + irb[d, 3, h].astype(F32)
        own_i[0, rows, :] = total

    f_s[...] = fdot(expd[...], own_i[0].astype(BF16)).reshape(NSP, CAPP, W).astype(BF16)
    j_r[sp] = f_s[sp]

    def j_send(k, _):
        sp_copy(k, f_s, j_r, j_ss, j_rs, True).start()
        return 0

    def j_wait(k, _):
        sp_copy(k, f_s, j_r, j_ss, j_rs, False).wait()
        return 0

    lax.fori_loop(1, NSP, j_send, 0)
    rows8 = jnp.concatenate(
        [slot_row(0).astype(F32), slot_row(1).astype(F32), rw_t[0:1, :], rw_t[1:2, :], jnp.zeros((4, TOK), F32)], axis=0
    )
    cols8[...] = jnp.transpose(rows8)
    final = hs[...].astype(F32) + scatter_end(own_s, pi_s, sb_s, rb_s, s_ss, s_rs)
    lax.fori_loop(1, NSP, j_wait, 0)
    back = j_r[...].astype(F32).reshape(PROWS, W).astype(BF16)
    for k in range(2):
        pick = onehot(iota((TOK, PROWS), 1) == cols8[:, k:k + 1].astype(jnp.int32))
        final = final + fdot(pick, back) * cols8[:, k + 2:k + 3]

    j16 = iota((NTP * OWNP, 1), 0)
    spread = onehot(iota((NTP * OWNP, TOK), 1) == jnp.where((j16 & 15) < OWN, OWN * (j16 >> 4) + (j16 & 15), -1))
    l_s[...] = fdot(spread, final.astype(BF16)).astype(BF16).reshape(NTP, OWNP, W)
    l_r[:, lanes(t, W)] = l_s[t]

    def l_copy(k, to):
        tt = lax.rem(t + k, NTP) if to else lax.rem(t + NTP - k, NTP)
        return rcopy(l_s.at[tt], l_r.at[:, lanes(t if to else tt, W)], l_ss.at[k], l_rs.at[k], tdev(tt))

    def l_send(k, _):
        l_copy(k, True).start()
        return 0

    def l_wait(k, _):
        l_copy(k, False).wait()
        return 0

    lax.fori_loop(1, NTP, l_send, 0)
    for off in range(1, NY):
        e_copy(off).wait_send()
    for off in range(NY):
        e_fwd(off, c).wait_send()
    z_ring.finish(False)
    y_ring.finish(True)
    for off in range(1, NX):
        q_copy(off, True).wait_send()
    for k in range(1, 5):
        for h in range(2):
            for d in range(2):
                if k > 1 or h == d:
                    i_copy(d, k, h).wait_send()
    lax.fori_loop(1, NTP, l_wait, 0)
    out[...] = l_r[0:OWN, :]


def layer(vmem_args, hbm_args):
    dma = pltpu.SemaphoreType.DMA
    vm = pltpu.VMEM
    row = vm((1, NX * TOK), F32)
    scratch = [
        vm((NZ, TOK, 640), BF16), vm((NX, TOK, 256), BF16), vm((VA + VB, 512), BF16), row, row, row, row,
        vm((VA, NX * TOK), F32), vm((VB, NX * TOK), F32), vm((NX, VA + VB, TOK), BF16), vm((NX, 8, TOK), F32),
        vm((NX, VA + VB, TOK), BF16), vm((NX, 8, TOK), F32), vm((TOK, VA + VB), BF16), vm((TOK, 8), F32),
        vm((VA + VB, D), BF16), vm((D, 2 * W), BF16), vm((W, D), BF16), vm((D, 2 * W), BF16), vm((W, D), BF16),
        vm((OWNP, D), BF16), vm((NTP, OWNP, W), BF16),
        vm((NY, TOK, W), F32), vm((NY, TOK, W), BF16), vm((NY, TOK, W), BF16), vm((NY, TOK, W), BF16), vm((NY, TOK, W), BF16),
        vm((TOK, W), BF16), vm((TOK, D), BF16), vm((TOK, D), BF16),
        vm((NY, TOK, W), BF16), vm((NY, TOK, W), BF16), vm((NY, TOK, W), BF16), vm((NY, TOK, W), BF16), vm((NY, TOK, W), F32),
        vm((NSP, CAPP, W), BF16), vm((NSP, CAPP, W), BF16), vm((ROWS, PROWS), BF16), vm((PROWS, ROWS), BF16), vm((NY, ROWS, 2 * W), BF16), vm((ROWS, 2 * W), F32),
        vm((NY, ROWS, W), F32), vm((NY, ROWS, W), BF16), vm((NY, ROWS, W), BF16), vm((2, 4, 2, HALF, W), BF16), vm((2, 4, 2, HALF, W), BF16),
        vm((NSP, CAPP, W), BF16), vm((NTP, OWNP, W), BF16), vm((OWNP, D), BF16),
    ] + [
        dma(n) for n in (
            (2, 4, 2), (2, 4, 2), (2, 4, 2), (2, 4, 2), (2,), (2,), (NX,), (NX,), (NX,), (NX,), (NX,), (NX,),
            (8,), (NTP,), (NTP,), (NY,), (NY,), (NY,), (NY,), (NY,), (NY,), (NY,), (NY,),
            (NY,), (NY,), (NY,), (NY,), (NSP,), (NSP,),
            (2, 4, 2), (2, 4, 2), (2, 4, 2), (2, 4, 2), (2,), (2,),
            (NY,), (NY,), (2, 4, 2), (2, 4, 2), (NSP,), (NSP,), (NTP,), (NTP,),
        )
    ]
    vspec = pl.BlockSpec(memory_space=pltpu.VMEM)
    hspec = pl.BlockSpec(memory_space=pl.ANY)
    return pl.pallas_call(
        layer_kernel,
        out_shape=jax.ShapeDtypeStruct((OWN, D), BF16),
        in_specs=[vspec] * len(vmem_args) + [hspec] * len(hbm_args),
        out_specs=vspec,
        scratch_shapes=scratch,
        compiler_params=pltpu.CompilerParams(collective_id=1, has_side_effects=True, vmem_limit_bytes=60 * 2**20),
        name="layer",
    )(*vmem_args, *hbm_args)


def tables(positions):
    freqs = theta_base ** (-(2.0 * jnp.arange(ROPE // 2, dtype=F32)) / ROPE)
    angles = positions.astype(F32)[:, None] * freqs[None, :]
    cosine, sine = jnp.cos(angles), jnp.sin(angles)
    return jnp.concatenate([cosine, cosine], axis=1), jnp.concatenate([-sine, sine], axis=1)


def shards(
    residual, query_a, query_b, latents, rope_key, key_up_a, value_up_a, key_up_b, value_up_b,
    out_proj_a, out_proj_b, norm_gain, routes, route_weights, shared_gate, shared_up, shared_down,
    expert_gate, expert_up, expert_down,
):
    first_row = lax.axis_index(SP) * TOK
    cosine, sine = tables(first_row + jnp.arange(TOK, dtype=jnp.int32))
    return layer(
        (
            query_a, query_b, latents, rope_key, cosine, sine, key_up_a, key_up_b, value_up_a, value_up_b,
            residual, norm_gain.reshape(1, D), routes.T, route_weights.T,
        ),
        (out_proj_a, out_proj_b, shared_gate, shared_up, shared_down, expert_gate[0], expert_up[0], expert_down[0]),
    )


def solution(mesh):
    torus = Mesh(mesh.devices.reshape(NZ, NX, NY, NC), ALL)
    rows, cols, split = P(SP, None), P(None, TP), P(TP, None)
    in_specs = (
        P(SP + TP, None), P(SP, TP), P(SP, TP), rows, rows, cols, cols, cols, cols, split, split, P(), rows, rows,
        cols, cols, split, P(SP, None, TP), P(SP, None, TP), P(SP, TP, None),
    )
    return jax.shard_map(
        shards, mesh=torus, in_specs=in_specs, out_specs=P(SP + TP, None), check_vma=False
    )
```

time: 247 us -> 145 us (0.59)
  waiting for transfers between devices: 93 us -> 0 us
  Pallas kernels: 105 us -> 137 us
  matrix products: 19.8 us -> 0 us
  between operations: 13.5 us -> 0.04 us
  other arithmetic: 5.3 us -> 0.17 us
  local copies, waits for them, and re-layouts: 10.2 us -> 6.94 us
    all_gather x1 -> x0, waiting for transfers between devices: 93 us -> none  [sent_together(): lax.all_gather(both, axis, axis=dim, tiled=True)]
    pallas_call x1, Pallas kernels: 105 us -> 137 us  [layer(): pl.pallas_call(layer_kernel, out_shape=jax.ShapeDtypeStruct((OWN, D), BF1...]
    dot_general x10 -> x0, matrix products: 19.8 us -> none  [the longest x2 8.34 us: group_update(): jnp.einsum('qhr,kr->hqk', queries_rope, rot_piece, preferred_element_type...]
    another operation x5 -> x0, other arithmetic: 3.17 us -> none
    unnamed x7 -> x13, local copies, waits for them, and re-layouts: 5.41 us -> 5.48 us
  transfers between devices with their start and end apart: 1 -> 0, of which waited for: 1 -> 0; matrix products, arithmetic and copies ran while one was open for 3% -> 0% of each run, Pallas kernels for 0% -> 0%
where the time goes in v2:
time: 145 us; the launch traced here: 144 us
  Pallas kernels  137 us (94%)
  local copies, waits for them, and re-layouts  6.94 us (5%)
    pallas_call x1, Pallas kernels, layer(): pl.pallas_call(layer_kernel, out_shape=jax.ShapeDtypeStruct((OWN, D), BF1...  137 us
    unnamed x13, local copies, waits for them, and re-layouts  5.48 us

profile of v2, /device:TPU:1, one launch (start us, length us, event | category | flops | bytes accessed | tf_op | source)
XLA Modules:
  0.0 144.2 jit_solution(15180486808493300727)
XLA Ops:
  0.0 0.1 fusion
  0.2 0.0 copy-start.3
  0.2 0.7 copy-done.3
  0.9 0.7 copy.26.rope
  1.6 0.7 copy.27.cosine
  2.3 0.0 copy-start
  2.3 0.7 copy.28.sine
  3.1 0.2 copy-done
  3.2 0.0 copy-start.1
  3.2 0.7 copy.25.qb
  4.0 0.1 copy-done.1
  4.1 0.0 copy-start.2
  4.1 0.7 copy.29.kua
  4.8 0.1 copy-done.2
  4.9 0.8 copy.30.vua
  5.7 137.1 %layer.1 = bf16[12,2048]{1,0:T(8,128)(2,1)} custom-call(bf16[192,96]{1,0:T(8,128)(2,1)} %qa.1, bf16[192,160]{1,0:T(8,128)(2,1)} %copy.25.qb, bf16[192,512]{1,0:T(8,128)(2,1)} %lat.1, bf16[192,32]{1,0:T(8,128)(2,1)} %copy.26.rope, f32[192,32]{1,0:T(8,128)} %copy.27.cosine, f32[192,32]{1,0:T(8,128)} %copy.28.sine, bf16[512,64]{1,0:T(8,128)(2,1)} %copy.29.kua, ...), custom_call_target="tpu_custom_call" | custom-call | tf_op jit(solution)/shard_map/layer/pallas_call | solution.py:596
  142.8 1.5 %copy.32 = bf16[12,2048]{1,0:T(8,128)(2,1)} copy(bf16[12,2048]{1,0:T(8,128)(2,1)} %layer.1) | data formatting | bytes 98304
  (3 shorter events, 0.0 us)
Async XLA Ops:
  0.2 0.7 copy-start.3
  2.3 0.9 copy-start
  3.2 0.8 copy-start.1
  4.1 0.8 copy-start.2

commit v3 on v2

--- a/solution.py
+++ b/solution.py
@@ -23,7 +23,9 @@
 NTP = NY * NC
 ROWS = NSP * CAP
 PROWS = NSP * CAPP
-HALF = ROWS // 2
+Z_PIECES = 2
+PIECES = 4
+PIECE = ROWS // PIECES
 OWN = TOK // NTP
 OWNP = 16
 SP = ("z", "x")
@@ -68,16 +70,16 @@
 
 
 def layer_kernel(
-    qa, qb, lat, rope, cosine, sine, kua, kub, vua, vub,
+    qa, qb_t, lat, rope_t, cosine, sine, kua_t, kub, vua_t, vub,
     resid, gain, routes_t, rw_t,
     oa_h, ob_h, sg_h, su_h, sd_h, eg_h, eu_h, ed_h,
     out,
     lz, q_all, wv_t, m_a, l_a, m_b, l_b, acc_a, acc_b, ps, st, pr, sr, heads, cols8,
     wo, sgu, sd, egu, ed,
     r_s, r_r, own_d, po_d, pi_d, sb_d, rb_d,
-    hs, hfull, normed,
+    hs, hidden,
     po_s, pi_s, sb_s, rb_s, own_s,
-    f_s, f_r, comp, expd, g, hacc,
+    f_s, f_r, tight, ssq, g, hacc,
     own_i, po_i, pi_i, isb, irb, j_r, l_s, l_r,
     z_ss, z_rs, zf_ss, zf_rs, zo_ss, zo_rs, q_ss, q_rs, x_ss, x_rs, t_ss, t_rs,
     w_sem, r_ss, r_rs, pd_ss, pd_rs, d_ss, d_rs, e_ss, e_rs, ef_ss, ef_rs,
@@ -109,8 +111,8 @@
         return lax.rem(y + off, NY)
 
     class Ring:
-        def __init__(self, pos, dev, win, sems):
-            self.pos, self.dev, self.win = pos, dev, win
+        def __init__(self, pos, dev, win, pieces, sems):
+            self.pos, self.dev, self.win, self.pieces = pos, dev, win, pieces
             self.ss, self.rs, self.fs, self.fr, self.os, self.orr = sems
 
         def src(self, d, k):
@@ -120,7 +122,7 @@
             return self.dev(self.src(1 - d, 1))
 
         def ok(self, k, d, h):
-            return k < 4 or h == d
+            return k < 4 or (k == 4 and (h < self.pieces // 2) == (d == 0))
 
         def send(self, d, k, h):
             win = self.win(self.src(d, k - 1), h, c)
@@ -138,37 +140,48 @@
             win = self.win(self.pos, h, core)
             return rcopy(win, win, self.os.at[h], self.orr.at[h], partner)
 
-        def run(self, use, own_too, before_use):
-            for h in range(2):
+        def pass_on(self, k, d, h):
+            if self.ok(k, d, h):
+                self.got(d, k, h).wait_recv()
+                if self.ok(k + 1, d, h):
+                    self.send(d, k + 1, h).start()
+                self.fwd(d, k, h, c).start()
+
+        def whole(self, d, k):
+            for h in range(self.pieces):
+                if self.ok(k, d, h):
+                    self.fwd(d, k, h, oc).wait_recv()
+
+        def run(self, use, own_too, after_start, before_use):
+            half = self.pieces // 2
+            for h in range(self.pieces):
                 for d in range(2):
                     self.send(d, 1, h).start()
                 if own_too:
                     self.own(h, c).start()
+            after_start()
             for k in range(1, 5):
-                for h in range(2):
+                for h in range(self.pieces):
                     for d in range(2):
-                        if self.ok(k, d, h):
-                            self.got(d, k, h).wait_recv()
-                            if self.ok(k + 1, d, h) and k < 4:
-                                self.send(d, k + 1, h).start()
-                            self.fwd(d, k, h, c).start()
-                if k == 1:
+                        self.pass_on(k, d, h)
+                    if k > 1 and h == half - 1:
+                        self.whole(0, k - 1)
+                        use(self.src(0, k - 1), False)
+                if k > 1:
+                    self.whole(1, k - 1)
+                    use(self.src(1, k - 1), False)
+                else:
                     before_use()
                     if own_too:
-                        for h in range(2):
+                        for h in range(self.pieces):
                             self.own(h, oc).wait_recv()
                     use(self.pos, True)
-                else:
-                    for d in range(2):
-                        for h in range(2):
-                            self.fwd(d, k - 1, h, oc).wait_recv()
-                        use(self.src(d, k - 1), False)
-            self.fwd(0, 4, 0, oc).wait_recv()
-            self.fwd(1, 4, 1, oc).wait_recv()
+            self.whole(0, 4)
+            self.whole(1, 4)
             use(self.src(0, 4), False)
 
         def finish(self, own_too):
-            for h in range(2):
+            for h in range(self.pieces):
                 if own_too:
                     self.own(h, c).wait_send()
                 for k in range(1, 5):
@@ -198,26 +211,23 @@
     lax.fori_loop(1, NTP, greet_t, 0)
     lax.fori_loop(1, NSP, greet_s, 0)
 
+    def unit(size):
+        return onehot(iota((size, size), 0) == iota((size, size), 1))
+
     def turn(value):
         wide = value.astype(F32)
-        swapped = jnp.concatenate([wide[:, ROPE // 2:], wide[:, 0:ROPE // 2]], axis=1)
-        return wide * cosine[...] + swapped * sine[...]
-
-    rot = turn(rope[...])
+        swapped = jnp.concatenate([wide[ROPE // 2:], wide[0:ROPE // 2]], axis=0)
+        return (wide * cosine[...] + swapped * sine[...]).astype(BF16)
+
+    unit_tok = unit(TOK)
+    rot = turn(rope_t[...])
     lz[z, :, 0:512] = lat[...]
-    lz[z, :, 512:640] = jnp.concatenate([jnp.zeros((TOK, 64), F32), rot, rot], axis=1).astype(BF16)
-    wide_a, wide_b = qa[...], qb[...]
-    q_all[x] = jnp.concatenate(
-        [
-            wide_b[:, 0:DB].astype(F32),
-            wide_a[:, 0:DA].astype(F32),
-            turn(wide_a[:, DA:DA + ROPE]),
-            turn(wide_b[:, DB:DB + ROPE]),
-        ],
-        axis=1,
-    ).astype(BF16)
-    wv_t[0:VB] = nt(onehot(iota((VB, VB), 0) == iota((VB, VB), 1)), vub[...]).astype(BF16)
-    wv_t[VB:VB + VA] = nt(onehot(iota((VA, VA), 0) == iota((VA, VA), 1)), vua[...]).astype(BF16)
+    lz[z, :, 512:640] = nt(unit_tok, jnp.concatenate([jnp.zeros((64, TOK), BF16), rot, rot], axis=0)).astype(BF16)
+    qa_t = nt(unit(DA + ROPE), qa[...]).astype(BF16)
+    q_t = jnp.concatenate([qb_t[0:DB], qa_t[0:DA], turn(qa_t[DA:DA + ROPE]), turn(qb_t[DB:DB + ROPE])], axis=0)
+    q_all[x] = nt(unit_tok, q_t).astype(BF16)
+    wv_t[0:VB] = nt(unit(VB), vub[...]).astype(BF16)
+    wv_t[VB:VB + VA] = vua_t[...]
 
     names_t = onehot((iota((128, TOK), 0) == routes_t[0:1, :]) | (iota((128, TOK), 0) == routes_t[1:2, :]))
     upper = onehot(iota((TOK, TOK), 0) < iota((TOK, TOK), 1))
@@ -228,14 +238,8 @@
         return routes_t[k:k + 1, :] * CAPP + rank.astype(jnp.int32)
 
     r_s[...] = jnp.zeros_like(r_s)
+    tight[ROWS:, :] = jnp.zeros((8, W), F32)
     r_s[0:OWN, :] = resid[...]
-
-    i_col = iota((ROWS, 1), 0)
-    comp[...] = onehot(iota((ROWS, PROWS), 1) == i_col + (CAPP - CAP) * ((i_col * 3641) >> 16))
-    j_col = iota((PROWS, 1), 0)
-    j_q = (j_col * 2731) >> 16
-    j_r0 = j_col - CAPP * j_q
-    expd[...] = onehot(iota((PROWS, ROWS), 1) == jnp.where(j_r0 < CAP, CAP * j_q + j_r0, -1))
 
     pl.semaphore_wait(barrier, NTP - 1 + NSP - 1)
 
@@ -273,6 +277,13 @@
                     sb[off] = (own[off] + pi[off].astype(F32)).astype(BF16)
                     y_copy(off, sb, rb, ss, rs).start()
 
+    def scatter_send(own, po, pi, sb, rb, pss, prs, ss, rs):
+        pair_wait(0, po, pi, pss, prs)
+        for off in FAR_FIRST[:-1]:
+            pair_wait(off, po, pi, pss, prs)
+            sb[off] = (own[off] + pi[off].astype(F32)).astype(BF16)
+            y_copy(off, sb, rb, ss, rs).start()
+
     def scatter_end(own, pi, sb, rb, ss, rs):
         total = own[0] + pi[0].astype(F32)
         for off in range(1, NY):
@@ -281,8 +292,9 @@
         return total
 
     def z_win(zz, h, core):
-        start = pl.multiple_of(core * (TOK // 2) + h * (TOK // 4), TOK // 4)
-        return lz.at[zz, pl.ds(start, TOK // 4), :]
+        size = TOK // 2 // Z_PIECES
+        start = pl.multiple_of(core * (TOK // 2) + h * size, size)
+        return lz.at[zz, pl.ds(start, size), :]
 
     def q_copy(off, to):
         src = x if to else lax.rem(x + NX - off, NX)
@@ -298,7 +310,7 @@
         part, twice = rows[:, 0:512], rows[:, 512:640].astype(F32)
         lane = iota((TOK, 128), 1)
         keys_b = fdot(part, kub[...])
-        keys_a = jnp.concatenate([fdot(part, kua[...]), twice[:, 64:128]], axis=1)
+        keys_a = jnp.concatenate([nt(part, kua_t[...]), twice[:, 64:128]], axis=1)
         keys_a = jnp.where(lane < 96, keys_a, 0.0).astype(BF16)
         keys_b = jnp.concatenate([keys_b, jnp.where(lane < 96, 0.0, twice)], axis=1).astype(BF16)
         values = nt(wv_t[...], part).astype(BF16)
@@ -330,10 +342,10 @@
         else:
             pl.when(zz < z)(lambda: block(zz, False))
 
-    z_ring = Ring(z, zdev, z_win, (z_ss, z_rs, zf_ss, zf_rs, zo_ss, zo_rs))
+    z_ring = Ring(z, zdev, z_win, Z_PIECES, (z_ss, z_rs, zf_ss, zf_rs, zo_ss, zo_rs))
     for off in (2, 1, 3):
         q_copy(off, True).start()
-    z_ring.run(use_block, False, queries_here)
+    z_ring.run(use_block, False, lambda: None, queries_here)
 
     share_b = jnp.where(l_b[...] > 0, 1.0 / l_b[...], 0.0)
     share_a = jnp.where(l_a[...] > 0, 1.0 / l_a[...], 0.0)
@@ -355,8 +367,13 @@
         x_copy(ps, pr, x_ss, x_rs, off, True).start()
     pr[x] = ps[x]
     sr[x] = st[x]
-    for load in loads[:2]:
+    for load in loads:
         load.wait()
+    for i in range(NTP):
+        cut = slice(i * W, (i + 1) * W)
+        column = jnp.transpose(jnp.broadcast_to(gain[:, cut], (8, W)))[:, 0:1]
+        for ref in (sgu, egu):
+            ref[cut, :] = (ref[cut, :].astype(F32) * column).astype(BF16)
     for off in range(1, NX):
         x_copy(st, sr, t_ss, t_rs, off, False).wait()
         x_copy(ps, pr, x_ss, x_rs, off, False).wait()
@@ -368,7 +385,7 @@
         whole = 1.0 / sum(part)
         merged.append(sum(pr[i, lo:hi].astype(F32) * (part[i] * whole) for i in range(NX)))
     turned = jnp.concatenate(merged, axis=0).astype(BF16)
-    heads[...] = nt(onehot(iota((TOK, TOK), 0) == iota((TOK, TOK), 1)), turned).astype(BF16)
+    heads[...] = nt(unit_tok, turned).astype(BF16)
 
     def head_cols(yy):
         return fdot(heads[...], wo[:, lanes(yy, 2 * W)])
@@ -386,80 +403,84 @@
     resid_cols = fdot(pick12, r_r[...].reshape(NTP * OWNP, W))
     hs[...] = (resid_cols + mixed).astype(BF16)
 
-    hfull[:, lanes(t, W)] = hs[...]
+    place = onehot((iota((PROWS, TOK), 0) == slot_row(0)) | (iota((PROWS, TOK), 0) == slot_row(1)))
+
+    f_s[...] = fdot(place, hs[...]).reshape(NSP, CAPP, W).astype(BF16)
+    f_r[sp] = f_s[sp]
+
+    def sp_copy(k, src, dst, ss, rs, to):
+        peer = lax.rem(sp + k, NSP) if to else lax.rem(sp + NSP - k, NSP)
+        return rcopy(src.at[peer], dst.at[sp if to else peer], ss.at[k], rs.at[k], sdev(peer))
+
+    def f_send(k, _):
+        sp_copy(k, f_s, f_r, f_ss, f_rs, True).start()
+        return 0
+
+    def f_wait(k, _):
+        sp_copy(k, f_s, f_r, f_ss, f_rs, False).wait()
+        return 0
+
+    lax.fori_loop(1, NSP, f_send, 0)
+
+    hidden[:, lanes(t, W)] = hs[...]
 
     def e_copy(off):
-        return rcopy(hs, hfull.at[:, lanes(t, W)], e_ss.at[off], e_rs.at[off], ydev(yoff(off)))
+        return rcopy(hs, hidden.at[:, lanes(t, W)], e_ss.at[off], e_rs.at[off], ydev(yoff(off)))
 
     def e_got(off):
         src = lanes(lax.rem(y + NY - off, NY) * NC + c, W)
-        return rcopy(hs, hfull.at[:, src], e_ss.at[off], e_rs.at[off], ydev(yoff(off)))
+        return rcopy(hs, hidden.at[:, src], e_ss.at[off], e_rs.at[off], ydev(yoff(off)))
 
     def e_fwd(off, core):
-        win = hfull.at[:, lanes(lax.rem(y + NY - off, NY) * NC + core, W)]
+        win = hidden.at[:, lanes(lax.rem(y + NY - off, NY) * NC + core, W)]
         return rcopy(win, win, ef_ss.at[off], ef_rs.at[off], partner)
 
     for off in FAR_FIRST[:-1]:
         e_copy(off).start()
     e_fwd(0, c).start()
-    for off in (1, 7, 2, 6, 3, 5, 4):
-        e_got(off).wait_recv()
-        e_fwd(off, c).start()
-    for off in range(NY):
-        e_fwd(off, oc).wait_recv()
-
-    def norm_rows(b, _):
-        rows = pl.ds(pl.multiple_of(b * 16, 16), 16)
-        wide = hfull[rows, :].astype(F32)
-        mean = jnp.mean(wide * wide, axis=-1, keepdims=True)
-        normed[rows, :] = (wide * lax.rsqrt(mean + norm_eps) * gain[...]).astype(BF16)
-        return 0
-
-    lax.fori_loop(0, TOK // 16, norm_rows, 0)
-
-    place = onehot((iota((PROWS, TOK), 0) == slot_row(0)) | (iota((PROWS, TOK), 0) == slot_row(1)))
-    f_s[...] = fdot(place, normed[:, lanes(t, W)]).reshape(NSP, CAPP, W).astype(BF16)
-    f_r[sp] = f_s[sp]
-
-    def sp_copy(k, src, dst, ss, rs, to):
-        peer = lax.rem(sp + k, NSP) if to else lax.rem(sp + NSP - k, NSP)
-        return rcopy(src.at[peer], dst.at[sp if to else peer], ss.at[k], rs.at[k], sdev(peer))
-
-    def f_send(k, _):
-        sp_copy(k, f_s, f_r, f_ss, f_rs, True).start()
-        return 0
-
-    def f_wait(k, _):
-        sp_copy(k, f_s, f_r, f_ss, f_rs, False).wait()
-        return 0
-
-    lax.fori_loop(1, NSP, f_send, 0)
-
-    for load in loads[2:]:
-        load.wait()
-    both = fdot(normed[...], sgu[...])
-    gate, up = both[:, 0:W], both[:, W:2 * W]
-    shared_act = (gate / (1.0 + jnp.exp(-gate)) * up).astype(BF16)
-
-    def shared_cols(yy):
-        return fdot(shared_act, sd[:, lanes(yy, 2 * W)])
-
-    scatter_start(shared_cols, own_s, po_s, pi_s, sb_s, rb_s, ps_ss, ps_rs, s_ss, s_rs)
-
     lax.fori_loop(1, NSP, f_wait, 0)
-    g[y, :, lanes(c, W)] = fdot(comp[...], f_r[...].astype(F32).reshape(PROWS, W).astype(BF16)).astype(BF16)
+    for e in range(NSP):
+        tight[e * CAP:e * CAP + CAPP, :] = f_r[e].astype(F32)
+    g[y, :, lanes(c, W)] = tight[0:ROWS, :].astype(BF16)
 
     def g_win(yy, h, core):
-        return g.at[yy, pl.ds(h * HALF, HALF), lanes(core, W)]
+        return g.at[yy, pl.ds(h * PIECE, PIECE), lanes(core, W)]
 
     def gate_up(yy, first):
+        wide = g[yy].astype(F32)
+        wide = wide * wide
+        squares = wide[:, 0:W] + wide[:, W:2 * W]
+        ssq[...] = squares if first else ssq[...] + squares
         value = fdot(g[yy], egu[pl.ds(pl.multiple_of(yy * 2 * W, 2 * W), 2 * W), :])
         hacc[...] = value if first else hacc[...] + value
 
-    y_ring = Ring(y, ydev, g_win, (g_ss, g_rs, gf_ss, gf_rs, go_ss, go_rs))
-    y_ring.run(gate_up, True, lambda: None)
-    gate, up = hacc[:, 0:W], hacc[:, W:2 * W]
-    act = (gate / (1.0 + jnp.exp(-gate)) * up).astype(BF16)
+    y_ring = Ring(y, ydev, g_win, PIECES, (g_ss, g_rs, gf_ss, gf_rs, go_ss, go_rs))
+    def hidden_relay():
+        for off in (1, 7, 2, 6, 3, 5, 4):
+            e_got(off).wait_recv()
+            e_fwd(off, c).start()
+
+    def root(total):
+        return lax.rsqrt(jnp.sum(total, axis=1, keepdims=True) * (1.0 / D) + norm_eps)
+
+    def gated(both, scale):
+        gate, up = both[:, 0:W] * scale, both[:, W:2 * W] * scale
+        return (gate / (1.0 + jnp.exp(-gate)) * up).astype(BF16)
+
+    def shared_pairs():
+        for off in range(NY):
+            e_fwd(off, oc).wait_recv()
+        total = jnp.zeros((TOK, W), F32)
+        for i in range(NTP):
+            wide = hidden[:, i * W:(i + 1) * W].astype(F32)
+            total = total + wide * wide
+        shared_act = gated(fdot(hidden[...], sgu[...]), root(total))
+        for off in range(NY):
+            value = fdot(shared_act, sd[:, lanes(yoff(off), 2 * W)])
+            pair_out(value, off, own_s, po_s, pi_s, ps_ss, ps_rs)
+
+    y_ring.run(gate_up, True, hidden_relay, shared_pairs)
+    act = gated(hacc[...], root(ssq[...]))
 
     def i_pair(off):
         pair_out(fdot(act, ed[:, lanes(yoff(off), 2 * W)]), off, own_i, po_i, pi_i, pp_ss, pp_rs)
@@ -467,14 +488,17 @@
     def i_copy(d, k, h):
         return rcopy(isb.at[d, k - 1, h], irb.at[d, k - 1, h], i_ss.at[d, k - 1, h], i_rs.at[d, k - 1, h], y_ring.to(d))
 
+    def i_ok(d, k, h):
+        return k > 1 or (h < PIECES // 2) == (d == 0)
+
     def i_step(k):
-        for h in range(2):
+        for h in range(PIECES):
             for d in range(2):
-                if k > 1 or h == d:
+                if i_ok(d, k, h):
                     off = (5 - k) if d == 0 else (3 + k)
-                    rows = pl.ds(h * HALF, HALF)
+                    rows = pl.ds(h * PIECE, PIECE)
                     total = own_i[off, rows, :] + pi_i[off, rows, :].astype(F32)
-                    if k > 2 or (k == 2 and h == d):
+                    if k > 1 and i_ok(d, k - 1, h):
                         i_copy(d, k - 1, h).wait_recv()
                         total = total + irb[d, k - 2, h].astype(F32)
                     isb[d, k - 1, h] = total.astype(BF16)
@@ -500,15 +524,16 @@
     pair_wait(7, po_i, pi_i, pp_ss, pp_rs)
     i_step(4)
     pair_wait(0, po_i, pi_i, pp_ss, pp_rs)
-    for h in range(2):
-        rows = pl.ds(h * HALF, HALF)
+    for h in range(PIECES):
+        rows = pl.ds(h * PIECE, PIECE)
         total = own_i[0, rows, :] + pi_i[0, rows, :].astype(F32)
         for d in range(2):
             i_copy(d, 4, h).wait_recv()
             total = total + irb[d, 3, h].astype(F32)
-        own_i[0, rows, :] = total
-
-    f_s[...] = fdot(expd[...], own_i[0].astype(BF16)).reshape(NSP, CAPP, W).astype(BF16)
+        tight[rows, :] = total
+
+    for e in range(NSP):
+        f_s[e] = tight[e * CAP:e * CAP + CAPP, :].astype(BF16)
     j_r[sp] = f_s[sp]
 
     def j_send(k, _):
@@ -520,6 +545,7 @@
         return 0
 
     lax.fori_loop(1, NSP, j_send, 0)
+    scatter_send(own_s, po_s, pi_s, sb_s, rb_s, ps_ss, ps_rs, s_ss, s_rs)
     rows8 = jnp.concatenate(
         [slot_row(0).astype(F32), slot_row(1).astype(F32), rw_t[0:1, :], rw_t[1:2, :], jnp.zeros((4, TOK), F32)], axis=0
     )
@@ -558,9 +584,9 @@
     for off in range(1, NX):
         q_copy(off, True).wait_send()
     for k in range(1, 5):
-        for h in range(2):
+        for h in range(PIECES):
             for d in range(2):
-                if k > 1 or h == d:
+                if i_ok(d, k, h):
                     i_copy(d, k, h).wait_send()
     lax.fori_loop(1, NTP, l_wait, 0)
     out[...] = l_r[0:OWN, :]
@@ -570,6 +596,7 @@
     dma = pltpu.SemaphoreType.DMA
     vm = pltpu.VMEM
     row = vm((1, NX * TOK), F32)
+    zsem, ysem = (2, 4, Z_PIECES), (2, 4, PIECES)
     scratch = [
         vm((NZ, TOK, 640), BF16), vm((NX, TOK, 256), BF16), vm((VA + VB, 512), BF16), row, row, row, row,
         vm((VA, NX * TOK), F32), vm((VB, NX * TOK), F32), vm((NX, VA + VB, TOK), BF16), vm((NX, 8, TOK), F32),
@@ -577,18 +604,18 @@
         vm((VA + VB, D), BF16), vm((D, 2 * W), BF16), vm((W, D), BF16), vm((D, 2 * W), BF16), vm((W, D), BF16),
         vm((OWNP, D), BF16), vm((NTP, OWNP, W), BF16),
         vm((NY, TOK, W), F32), vm((NY, TOK, W), BF16), vm((NY, TOK, W), BF16), vm((NY, TOK, W), BF16), vm((NY, TOK, W), BF16),
-        vm((TOK, W), BF16), vm((TOK, D), BF16), vm((TOK, D), BF16),
+        vm((TOK, W), BF16), vm((TOK, D), BF16),
         vm((NY, TOK, W), BF16), vm((NY, TOK, W), BF16), vm((NY, TOK, W), BF16), vm((NY, TOK, W), BF16), vm((NY, TOK, W), F32),
-        vm((NSP, CAPP, W), BF16), vm((NSP, CAPP, W), BF16), vm((ROWS, PROWS), BF16), vm((PROWS, ROWS), BF16), vm((NY, ROWS, 2 * W), BF16), vm((ROWS, 2 * W), F32),
-        vm((NY, ROWS, W), F32), vm((NY, ROWS, W), BF16), vm((NY, ROWS, W), BF16), vm((2, 4, 2, HALF, W), BF16), vm((2, 4, 2, HALF, W), BF16),
+        vm((NSP, CAPP, W), BF16), vm((NSP, CAPP, W), BF16), vm((ROWS + 8, W), F32), vm((ROWS, W), F32), vm((NY, ROWS, 2 * W), BF16), vm((ROWS, 2 * W), F32),
+        vm((NY, ROWS, W), F32), vm((NY, ROWS, W), BF16), vm((NY, ROWS, W), BF16), vm((2, 4, PIECES, PIECE, W), BF16), vm((2, 4, PIECES, PIECE, W), BF16),
         vm((NSP, CAPP, W), BF16), vm((NTP, OWNP, W), BF16), vm((OWNP, D), BF16),
     ] + [
         dma(n) for n in (
-            (2, 4, 2), (2, 4, 2), (2, 4, 2), (2, 4, 2), (2,), (2,), (NX,), (NX,), (NX,), (NX,), (NX,), (NX,),
+            zsem, zsem, zsem, zsem, (2,), (2,), (NX,), (NX,), (NX,), (NX,), (NX,), (NX,),
             (8,), (NTP,), (NTP,), (NY,), (NY,), (NY,), (NY,), (NY,), (NY,), (NY,), (NY,),
             (NY,), (NY,), (NY,), (NY,), (NSP,), (NSP,),
-            (2, 4, 2), (2, 4, 2), (2, 4, 2), (2, 4, 2), (2,), (2,),
-            (NY,), (NY,), (2, 4, 2), (2, 4, 2), (NSP,), (NSP,), (NTP,), (NTP,),
+            ysem, ysem, ysem, ysem, (PIECES,), (PIECES,),
+            (NY,), (NY,), ysem, ysem, (NSP,), (NSP,), (NTP,), (NTP,),
         )
     ]
     vspec = pl.BlockSpec(memory_space=pltpu.VMEM)
@@ -606,9 +633,9 @@
 
 def tables(positions):
     freqs = theta_base ** (-(2.0 * jnp.arange(ROPE // 2, dtype=F32)) / ROPE)
-    angles = positions.astype(F32)[:, None] * freqs[None, :]
+    angles = positions.astype(F32)[None, :] * freqs[:, None]
     cosine, sine = jnp.cos(angles), jnp.sin(angles)
-    return jnp.concatenate([cosine, cosine], axis=1), jnp.concatenate([-sine, sine], axis=1)
+    return jnp.concatenate([cosine, cosine], axis=0), jnp.concatenate([-sine, sine], axis=0)
 
 
 def shards(
@@ -620,7 +647,7 @@
     cosine, sine = tables(first_row + jnp.arange(TOK, dtype=jnp.int32))
     return layer(
         (
-            query_a, query_b, latents, rope_key, cosine, sine, key_up_a, key_up_b, value_up_a, value_up_b,
+            query_a, query_b.T, latents, rope_key.T, cosine, sine, key_up_a.T, key_up_b, value_up_a.T, value_up_b,
             residual, norm_gain.reshape(1, D), routes.T, route_weights.T,
         ),
         (out_proj_a, out_proj_b, shared_gate, shared_up, shared_down, expert_gate[0], expert_up[0], expert_down[0]),

time: 145 us -> 124 us (0.86)
  Pallas kernels: 137 us -> 122 us
  local copies, waits for them, and re-layouts: 6.94 us -> 1.47 us
    pallas_call x1, Pallas kernels: 137 us -> 122 us  [layer(): pl.pallas_call(layer_kernel, out_shape=jax.ShapeDtypeStruct((OWN, D), BF1...]
    unnamed x13 -> x1, local copies, waits for them, and re-layouts: 5.48 us -> 1.47 us
    concatenate x2 -> x0, local copies, waits for them, and re-layouts: 1.46 us -> none  [the longest x1 0.73 us: tables(): jnp.concatenate([-sine, sine], axis=1)]
where the time goes in v3:
time: 124 us
  Pallas kernels  122 us (98%)
  local copies, waits for them, and re-layouts  1.47 us (1%)
    pallas_call x1, Pallas kernels, layer(): pl.pallas_call(layer_kernel, out_shape=jax.ShapeDtypeStruct((OWN, D), BF1...  122 us

profile of v3, /device:TPU:1, one launch (start us, length us, event | category | flops | bytes accessed | tf_op | source)
XLA Modules:
  0.0 124.0 jit_solution(9596189586881662171)
XLA Ops:
  0.0 0.1 fusion
  0.2 0.6 pad_maximum_fusion
  0.8 121.7 %layer.1 = bf16[12,2048]{1,0:T(8,128)(2,1)} custom-call(bf16[192,96]{1,0:T(8,128)(2,1)} %qa.1, bf16[160,192]{1,0:T(8,128)(2,1)} %bitcast.13, bf16[192,512]{1,0:T(8,128)(2,1)} %lat.1, bf16[32,192]{1,0:T(8,128)(2,1)} %bitcast.16, f32[32,192]{1,0:T(8,128)} %get-tuple-element.8.cosine, f32[32,192]{1,0:T(8,128)} %get-tuple-element.9.sine, ...), custom_call_target="tpu_custom_call" | custom-call | tf_op jit(solution)/shard_map/layer/pallas_call | solution.py:623
  122.5 1.5 %copy.22 = bf16[12,2048]{1,0:T(8,128)(2,1)} copy(bf16[12,2048]{1,0:T(8,128)(2,1)} %layer.1) | data formatting | bytes 98304
  (2 shorter events, 0.0 us)

commit v4 on v3

--- a/solution.py
+++ b/solution.py
@@ -35,6 +35,7 @@
 F32 = jnp.float32
 BF16 = jnp.bfloat16
 FAR_FIRST = (4, 3, 5, 2, 6, 1, 7, 0)
+MERGED = (4, 2, 6, 1, 7, 3, 5, 0)
 
 theta_base = 10000.0
 norm_eps = 1e-06
@@ -81,13 +82,16 @@
     po_s, pi_s, sb_s, rb_s, own_s,
     f_s, f_r, tight, ssq, g, hacc,
     own_i, po_i, pi_i, isb, irb, j_r, l_s, l_r,
+    f2_s, f2_r, j2_r, l2_s, l2_r, mg_d, mg_s,
     z_ss, z_rs, zf_ss, zf_rs, zo_ss, zo_rs, q_ss, q_rs, x_ss, x_rs, t_ss, t_rs,
     w_sem, r_ss, r_rs, pd_ss, pd_rs, d_ss, d_rs, e_ss, e_rs, ef_ss, ef_rs,
     ps_ss, ps_rs, s_ss, s_rs, f_ss, f_rs, g_ss, g_rs, gf_ss, gf_rs, go_ss, go_rs,
     pp_ss, pp_rs, i_ss, i_rs, j_ss, j_rs, l_ss, l_rs,
+    f2_ss, f2_rs, j2_ss, j2_rs, l2_ss, l2_rs, md_ss, md_rs, ms_ss, ms_rs, g4_ss, g4_rs,
 ):
     z, x, y, c = (lax.axis_index(a) for a in ALL)
     t = y * NC + c
+    t4 = lax.rem(y + 4, NY) * NC + c
     sp = z * NX + x
     oc = 1 - c
     partner = (z, x, y, oc)
@@ -111,7 +115,8 @@
         return lax.rem(y + off, NY)
 
     class Ring:
-        def __init__(self, pos, dev, win, pieces, sems):
+        def __init__(self, pos, dev, win, pieces, sems, short=False):
+            self.short = short
             self.pos, self.dev, self.win, self.pieces = pos, dev, win, pieces
             self.ss, self.rs, self.fs, self.fr, self.os, self.orr = sems
 
@@ -122,7 +127,7 @@
             return self.dev(self.src(1 - d, 1))
 
         def ok(self, k, d, h):
-            return k < 4 or (k == 4 and (h < self.pieces // 2) == (d == 0))
+            return k < 4 or (k == 4 and not self.short and (h < self.pieces // 2) == (d == 0))
 
         def send(self, d, k, h):
             win = self.win(self.src(d, k - 1), h, c)
@@ -152,7 +157,7 @@
                 if self.ok(k, d, h):
                     self.fwd(d, k, h, oc).wait_recv()
 
-        def run(self, use, own_too, after_start, before_use):
+        def run(self, use, own_too, after_start, before_use, fourth=None, fourth_end=None):
             half = self.pieces // 2
             for h in range(self.pieces):
                 for d in range(2):
@@ -161,6 +166,8 @@
                     self.own(h, c).start()
             after_start()
             for k in range(1, 5):
+                if k == 4 and self.short:
+                    fourth()
                 for h in range(self.pieces):
                     for d in range(2):
                         self.pass_on(k, d, h)
@@ -176,8 +183,11 @@
                         for h in range(self.pieces):
                             self.own(h, oc).wait_recv()
                     use(self.pos, True)
-            self.whole(0, 4)
-            self.whole(1, 4)
+            if self.short:
+                fourth_end()
+            else:
+                self.whole(0, 4)
+                self.whole(1, 4)
             use(self.src(0, 4), False)
 
         def finish(self, own_too):
@@ -265,28 +275,43 @@
     def y_copy(off, sb, rb, ss, rs):
         return rcopy(sb.at[off], rb.at[off], ss.at[off], rs.at[off], ydev(yoff(off)))
 
-    def scatter_start(cols, own, po, pi, sb, rb, pss, prs, ss, rs, lead=3):
+    def merge_copy(i, sb, mg, ms, mr):
+        half = sb.at[4, pl.ds(i * (TOK // 2), TOK // 2), :]
+        return rcopy(half, mg.at[i], ms.at[i], mr.at[i], ydev(yoff(1 if i == 0 else 7)))
+
+    def scatter_one(off, own, po, pi, sb, rb, pss, prs, ss, rs, mg, ms, mr):
+        pair_wait(off, po, pi, pss, prs)
+        if off == 0:
+            return
+        total = own[off] + pi[off].astype(F32)
+        if off in (3, 5):
+            i = 0 if off == 3 else 1
+            merge_copy(i, sb, mg, ms, mr).wait()
+            came = mg[i].astype(F32)
+            still = jnp.zeros_like(came)
+            total = total + jnp.concatenate([came, still] if i == 0 else [still, came], axis=0)
+        sb[off] = total.astype(BF16)
+        if off == 4:
+            for i in range(2):
+                merge_copy(i, sb, mg, ms, mr).start()
+        else:
+            y_copy(off, sb, rb, ss, rs).start()
+
+    def scatter_start(cols, own, po, pi, *rest, lead=3):
         for n in range(NY + lead):
             if n < NY:
-                off = FAR_FIRST[n]
-                pair_out(cols(yoff(off)), off, own, po, pi, pss, prs)
+                off = MERGED[n]
+                pair_out(cols(yoff(off)), off, own, po, pi, rest[2], rest[3])
             if n >= lead:
-                off = FAR_FIRST[n - lead]
-                pair_wait(off, po, pi, pss, prs)
-                if off:
-                    sb[off] = (own[off] + pi[off].astype(F32)).astype(BF16)
-                    y_copy(off, sb, rb, ss, rs).start()
-
-    def scatter_send(own, po, pi, sb, rb, pss, prs, ss, rs):
-        pair_wait(0, po, pi, pss, prs)
-        for off in FAR_FIRST[:-1]:
-            pair_wait(off, po, pi, pss, prs)
-            sb[off] = (own[off] + pi[off].astype(F32)).astype(BF16)
-            y_copy(off, sb, rb, ss, rs).start()
+                scatter_one(MERGED[n - lead], own, po, pi, *rest)
+
+    def scatter_send(offs, *all_of):
+        for off in offs:
+            scatter_one(off, *all_of)
 
     def scatter_end(own, pi, sb, rb, ss, rs):
         total = own[0] + pi[0].astype(F32)
-        for off in range(1, NY):
+        for off in (2, 6, 1, 7, 3, 5):
             y_copy(off, sb, rb, ss, rs).wait()
             total = total + rb[off].astype(F32)
         return total
@@ -390,7 +415,7 @@
     def head_cols(yy):
         return fdot(heads[...], wo[:, lanes(yy, 2 * W)])
 
-    scatter_start(head_cols, own_d, po_d, pi_d, sb_d, rb_d, pd_ss, pd_rs, d_ss, d_rs)
+    scatter_start(head_cols, own_d, po_d, pi_d, sb_d, rb_d, pd_ss, pd_rs, d_ss, d_rs, mg_d, md_ss, md_rs)
 
     def resid_wait(k, _):
         resid_copy(k, False).wait()
@@ -438,6 +463,15 @@
     for off in FAR_FIRST[:-1]:
         e_copy(off).start()
     e_fwd(0, c).start()
+
+    def f2_send(k, _):
+        sp_copy(k, f2_s, f2_r, f2_ss, f2_rs, True).start()
+        return 0
+
+    def f2_wait(k, _):
+        sp_copy(k, f2_s, f2_r, f2_ss, f2_rs, False).wait()
+        return 0
+
     lax.fori_loop(1, NSP, f_wait, 0)
     for e in range(NSP):
         tight[e * CAP:e * CAP + CAPP, :] = f_r[e].astype(F32)
@@ -454,9 +488,14 @@
         value = fdot(g[yy], egu[pl.ds(pl.multiple_of(yy * 2 * W, 2 * W), 2 * W), :])
         hacc[...] = value if first else hacc[...] + value
 
-    y_ring = Ring(y, ydev, g_win, PIECES, (g_ss, g_rs, gf_ss, gf_rs, go_ss, go_rs))
+    y_ring = Ring(y, ydev, g_win, PIECES, (g_ss, g_rs, gf_ss, gf_rs, go_ss, go_rs), True)
     def hidden_relay():
-        for off in (1, 7, 2, 6, 3, 5, 4):
+        e_got(4).wait_recv()
+        f2_s[...] = fdot(place, hidden[:, lanes(t4, W)]).reshape(NSP, CAPP, W).astype(BF16)
+        f2_r[sp] = f2_s[sp]
+        lax.fori_loop(1, NSP, f2_send, 0)
+        e_fwd(4, c).start()
+        for off in (1, 7, 2, 6, 3, 5):
             e_got(off).wait_recv()
             e_fwd(off, c).start()
 
@@ -479,7 +518,19 @@
             value = fdot(shared_act, sd[:, lanes(yoff(off), 2 * W)])
             pair_out(value, off, own_s, po_s, pi_s, ps_ss, ps_rs)
 
-    y_ring.run(gate_up, True, hidden_relay, shared_pairs)
+    def g_four(core):
+        win = g.at[yoff(4), :, lanes(core, W)]
+        return rcopy(win, win, g4_ss, g4_rs, partner)
+
+    def fourth():
+        lax.fori_loop(1, NSP, f2_wait, 0)
+        for e in range(NSP):
+            tight[e * CAP:e * CAP + CAPP, :] = f2_r[e].astype(F32)
+        g[yoff(4), :, lanes(c, W)] = tight[0:ROWS, :].astype(BF16)
+        g_four(c).start()
+        scatter_send((4, 2, 6), own_s, po_s, pi_s, sb_s, rb_s, ps_ss, ps_rs, s_ss, s_rs, mg_s, ms_ss, ms_rs)
+
+    y_ring.run(gate_up, True, hidden_relay, shared_pairs, fourth, lambda: g_four(oc).wait_recv())
     act = gated(hacc[...], root(ssq[...]))
 
     def i_pair(off):
@@ -487,49 +538,59 @@
 
     def i_copy(d, k, h):
         return rcopy(isb.at[d, k - 1, h], irb.at[d, k - 1, h], i_ss.at[d, k - 1, h], i_rs.at[d, k - 1, h], y_ring.to(d))
-
-    def i_ok(d, k, h):
-        return k > 1 or (h < PIECES // 2) == (d == 0)
 
     def i_step(k):
         for h in range(PIECES):
             for d in range(2):
-                if i_ok(d, k, h):
-                    off = (5 - k) if d == 0 else (3 + k)
-                    rows = pl.ds(h * PIECE, PIECE)
-                    total = own_i[off, rows, :] + pi_i[off, rows, :].astype(F32)
-                    if k > 1 and i_ok(d, k - 1, h):
-                        i_copy(d, k - 1, h).wait_recv()
-                        total = total + irb[d, k - 2, h].astype(F32)
-                    isb[d, k - 1, h] = total.astype(BF16)
-                    i_copy(d, k, h).start()
-
-    i_pair(4)
+                off = (4 - k) if d == 0 else (4 + k)
+                rows = pl.ds(h * PIECE, PIECE)
+                total = own_i[off, rows, :] + pi_i[off, rows, :].astype(F32)
+                if k > 1:
+                    i_copy(d, k - 1, h).wait_recv()
+                    total = total + irb[d, k - 2, h].astype(F32)
+                isb[d, k - 1, h] = total.astype(BF16)
+                i_copy(d, k, h).start()
+
+    def i_wait(*offs):
+        for off in offs:
+            pair_wait(off, po_i, pi_i, pp_ss, pp_rs)
+
     i_pair(3)
     i_pair(5)
-    pair_wait(4, po_i, pi_i, pp_ss, pp_rs)
+    i_pair(4)
+    i_pair(2)
+    i_wait(3, 5)
     i_step(1)
-    i_pair(2)
     i_pair(6)
-    pair_wait(3, po_i, pi_i, pp_ss, pp_rs)
-    pair_wait(5, po_i, pi_i, pp_ss, pp_rs)
+    i_wait(4)
+    tight[0:ROWS, :] = own_i[4] + pi_i[4].astype(F32)
+    for e in range(NSP):
+        f2_s[e] = tight[e * CAP:e * CAP + CAPP, :].astype(BF16)
+    j2_r[sp] = f2_s[sp]
+
+    def j2_send(k, _):
+        sp_copy(k, f2_s, j2_r, j2_ss, j2_rs, True).start()
+        return 0
+
+    def j2_wait(k, _):
+        sp_copy(k, f2_s, j2_r, j2_ss, j2_rs, False).wait()
+        return 0
+
+    lax.fori_loop(1, NSP, j2_send, 0)
+    i_wait(2, 6)
     i_step(2)
     i_pair(1)
     i_pair(7)
     i_pair(0)
-    pair_wait(2, po_i, pi_i, pp_ss, pp_rs)
-    pair_wait(6, po_i, pi_i, pp_ss, pp_rs)
+    i_wait(1, 7)
     i_step(3)
-    pair_wait(1, po_i, pi_i, pp_ss, pp_rs)
-    pair_wait(7, po_i, pi_i, pp_ss, pp_rs)
-    i_step(4)
-    pair_wait(0, po_i, pi_i, pp_ss, pp_rs)
+    i_wait(0)
     for h in range(PIECES):
         rows = pl.ds(h * PIECE, PIECE)
         total = own_i[0, rows, :] + pi_i[0, rows, :].astype(F32)
         for d in range(2):
-            i_copy(d, 4, h).wait_recv()
-            total = total + irb[d, 3, h].astype(F32)
+            i_copy(d, 3, h).wait_recv()
+            total = total + irb[d, 2, h].astype(F32)
         tight[rows, :] = total
 
     for e in range(NSP):
@@ -545,51 +606,65 @@
         return 0
 
     lax.fori_loop(1, NSP, j_send, 0)
-    scatter_send(own_s, po_s, pi_s, sb_s, rb_s, ps_ss, ps_rs, s_ss, s_rs)
+    scatter_send((3, 5, 1, 7, 0), own_s, po_s, pi_s, sb_s, rb_s, ps_ss, ps_rs, s_ss, s_rs, mg_s, ms_ss, ms_rs)
     rows8 = jnp.concatenate(
         [slot_row(0).astype(F32), slot_row(1).astype(F32), rw_t[0:1, :], rw_t[1:2, :], jnp.zeros((4, TOK), F32)], axis=0
     )
     cols8[...] = jnp.transpose(rows8)
+    j16 = iota((NTP * OWNP, 1), 0)
+    spread = onehot(iota((NTP * OWNP, TOK), 1) == jnp.where((j16 & 15) < OWN, OWN * (j16 >> 4) + (j16 & 15), -1))
+    picks = [onehot(iota((TOK, PROWS), 1) == cols8[:, k:k + 1].astype(jnp.int32)) for k in range(2)]
+
+    def routed(ref):
+        back = ref[...].astype(F32).reshape(PROWS, W).astype(BF16)
+        return sum(fdot(picks[k], back) * cols8[:, k + 2:k + 3] for k in range(2))
+
+    def to_rows(value, l_s, l_r, window, ss, rs):
+        l_s[...] = fdot(spread, value.astype(BF16)).astype(BF16).reshape(NTP, OWNP, W)
+        l_r[:, lanes(window(t), W)] = l_s[t]
+
+        def l_send(k, _):
+            l_copy(k, True, l_s, l_r, window, ss, rs).start()
+            return 0
+
+        lax.fori_loop(1, NTP, l_send, 0)
+
+    def l_copy(k, to, l_s, l_r, window, ss, rs):
+        tt = lax.rem(t + k, NTP) if to else lax.rem(t + NTP - k, NTP)
+        return rcopy(l_s.at[tt], l_r.at[:, lanes(window(t if to else tt), W)], ss.at[k], rs.at[k], tdev(tt))
+
+    def near(tt):
+        return tt
+
+    def far(tt):
+        return lax.rem(tt + NTP // 2, NTP)
+
+    lax.fori_loop(1, NSP, j2_wait, 0)
+    to_rows(routed(j2_r), l2_s, l2_r, far, l2_ss, l2_rs)
     final = hs[...].astype(F32) + scatter_end(own_s, pi_s, sb_s, rb_s, s_ss, s_rs)
     lax.fori_loop(1, NSP, j_wait, 0)
-    back = j_r[...].astype(F32).reshape(PROWS, W).astype(BF16)
-    for k in range(2):
-        pick = onehot(iota((TOK, PROWS), 1) == cols8[:, k:k + 1].astype(jnp.int32))
-        final = final + fdot(pick, back) * cols8[:, k + 2:k + 3]
-
-    j16 = iota((NTP * OWNP, 1), 0)
-    spread = onehot(iota((NTP * OWNP, TOK), 1) == jnp.where((j16 & 15) < OWN, OWN * (j16 >> 4) + (j16 & 15), -1))
-    l_s[...] = fdot(spread, final.astype(BF16)).astype(BF16).reshape(NTP, OWNP, W)
-    l_r[:, lanes(t, W)] = l_s[t]
-
-    def l_copy(k, to):
-        tt = lax.rem(t + k, NTP) if to else lax.rem(t + NTP - k, NTP)
-        return rcopy(l_s.at[tt], l_r.at[:, lanes(t if to else tt, W)], l_ss.at[k], l_rs.at[k], tdev(tt))
-
-    def l_send(k, _):
-        l_copy(k, True).start()
-        return 0
+    to_rows(final + routed(j_r), l_s, l_r, near, l_ss, l_rs)
 
     def l_wait(k, _):
-        l_copy(k, False).wait()
-        return 0
-
-    lax.fori_loop(1, NTP, l_send, 0)
+        l_copy(k, False, l2_s, l2_r, far, l2_ss, l2_rs).wait()
+        l_copy(k, False, l_s, l_r, near, l_ss, l_rs).wait()
+        return 0
+
     for off in range(1, NY):
         e_copy(off).wait_send()
     for off in range(NY):
         e_fwd(off, c).wait_send()
     z_ring.finish(False)
+    g_four(c).wait_send()
     y_ring.finish(True)
     for off in range(1, NX):
         q_copy(off, True).wait_send()
-    for k in range(1, 5):
+    for k in range(1, 4):
         for h in range(PIECES):
             for d in range(2):
-                if i_ok(d, k, h):
-                    i_copy(d, k, h).wait_send()
+                i_copy(d, k, h).wait_send()
     lax.fori_loop(1, NTP, l_wait, 0)
-    out[...] = l_r[0:OWN, :]
+    out[...] = (l_r[0:OWN, :].astype(F32) + l2_r[0:OWN, :].astype(F32)).astype(BF16)
 
 
 def layer(vmem_args, hbm_args):
@@ -609,6 +684,8 @@
         vm((NSP, CAPP, W), BF16), vm((NSP, CAPP, W), BF16), vm((ROWS + 8, W), F32), vm((ROWS, W), F32), vm((NY, ROWS, 2 * W), BF16), vm((ROWS, 2 * W), F32),
         vm((NY, ROWS, W), F32), vm((NY, ROWS, W), BF16), vm((NY, ROWS, W), BF16), vm((2, 4, PIECES, PIECE, W), BF16), vm((2, 4, PIECES, PIECE, W), BF16),
         vm((NSP, CAPP, W), BF16), vm((NTP, OWNP, W), BF16), vm((OWNP, D), BF16),
+        vm((NSP, CAPP, W), BF16), vm((NSP, CAPP, W), BF16), vm((NSP, CAPP, W), BF16), vm((NTP, OWNP, W), BF16), vm((OWNP, D), BF16),
+        vm((2, TOK // 2, W), BF16), vm((2, TOK // 2, W), BF16),
     ] + [
         dma(n) for n in (
             zsem, zsem, zsem, zsem, (2,), (2,), (NX,), (NX,), (NX,), (NX,), (NX,), (NX,),
@@ -616,8 +693,9 @@
             (NY,), (NY,), (NY,), (NY,), (NSP,), (NSP,),
             ysem, ysem, ysem, ysem, (PIECES,), (PIECES,),
             (NY,), (NY,), ysem, ysem, (NSP,), (NSP,), (NTP,), (NTP,),
+            (NSP,), (NSP,), (NSP,), (NSP,), (NTP,), (NTP,), (2,), (2,), (2,), (2,),
         )
-    ]
+    ] + [dma, dma]
     vspec = pl.BlockSpec(memory_space=pltpu.VMEM)
     hspec = pl.BlockSpec(memory_space=pl.ANY)
     return pl.pallas_call(

time: 124 us -> 118 us (0.952)
  Pallas kernels: 122 us -> 116 us
    pallas_call x1, Pallas kernels: 122 us -> 116 us  [layer(): pl.pallas_call(layer_kernel, out_shape=jax.ShapeDtypeStruct((OWN, D), BF1...]
where the time goes in v4:
time: 118 us
  Pallas kernels  116 us (98%)
  local copies, waits for them, and re-layouts  1.47 us (1%)
    pallas_call x1, Pallas kernels, layer(): pl.pallas_call(layer_kernel, out_shape=jax.ShapeDtypeStruct((OWN, D), BF1...  116 us

profile of v4, /device:TPU:1, one launch (start us, length us, event | category | flops | bytes accessed | tf_op | source)
XLA Modules:
  0.0 118.0 jit_solution(6584384805456624301)
XLA Ops:
  0.0 0.1 fusion
  0.2 0.6 pad_maximum_fusion
  0.8 115.8 %layer.1 = bf16[12,2048]{1,0:T(8,128)(2,1)} custom-call(bf16[192,96]{1,0:T(8,128)(2,1)} %qa.1, bf16[160,192]{1,0:T(8,128)(2,1)} %bitcast.13, bf16[192,512]{1,0:T(8,128)(2,1)} %lat.1, bf16[32,192]{1,0:T(8,128)(2,1)} %bitcast.16, f32[32,192]{1,0:T(8,128)} %get-tuple-element.8.cosine, f32[32,192]{1,0:T(8,128)} %get-tuple-element.9.sine, ...), custom_call_target="tpu_custom_call" | custom-call | tf_op jit(solution)/shard_map/layer/pallas_call | solution.py:701
  116.6 1.5 %copy.22 = bf16[12,2048]{1,0:T(8,128)(2,1)} copy(bf16[12,2048]{1,0:T(8,128)(2,1)} %layer.1) | data formatting | bytes 98304
  (2 shorter events, 0.0 us)

commit v5 on v4

--- a/solution.py
+++ b/solution.py
@@ -23,7 +23,7 @@
 NTP = NY * NC
 ROWS = NSP * CAP
 PROWS = NSP * CAPP
-Z_PIECES = 2
+Z_PIECES = 3
 PIECES = 4
 PIECE = ROWS // PIECES
 OWN = TOK // NTP
@@ -74,7 +74,7 @@
     qa, qb_t, lat, rope_t, cosine, sine, kua_t, kub, vua_t, vub,
     resid, gain, routes_t, rw_t,
     oa_h, ob_h, sg_h, su_h, sd_h, eg_h, eu_h, ed_h,
-    out,
+    out_near, out_far,
     lz, q_all, wv_t, m_a, l_a, m_b, l_b, acc_a, acc_b, ps, st, pr, sr, heads, cols8,
     wo, sgu, sd, egu, ed,
     r_s, r_r, own_d, po_d, pi_d, sb_d, rb_d,
@@ -374,11 +374,12 @@
 
     share_b = jnp.where(l_b[...] > 0, 1.0 / l_b[...], 0.0)
     share_a = jnp.where(l_a[...] > 0, 1.0 / l_a[...], 0.0)
-    out_b, out_a = (acc_b[...] * share_b).astype(BF16), (acc_a[...] * share_a).astype(BF16)
+    out = jnp.concatenate([acc_b[...] * share_b, acc_a[...] * share_a], axis=0).astype(BF16)
     for xx in range(NX):
         cut = slice(xx * TOK, (xx + 1) * TOK)
-        ps[xx, 0:VB] = out_b[:, cut]
-        ps[xx, VB:VB + VA] = out_a[:, cut]
+        one = out[:, cut]
+        ps[xx, 0:TOK] = one[:, 0:128]
+        ps[xx, TOK:] = jnp.concatenate([one[0:TOK // 2, 128:], one[TOK // 2:, 128:]], axis=1)
         for i, stat in enumerate((m_b, l_b, m_a, l_a)):
             st[xx, i:i + 1, :] = stat[:, cut]
             st[xx, i + 4:i + 5, :] = stat[:, cut]
@@ -402,13 +403,18 @@
     for off in range(1, NX):
         x_copy(st, sr, t_ss, t_rs, off, False).wait()
         x_copy(ps, pr, x_ss, x_rs, off, False).wait()
+    whole_of = []
+    for i in range(NX):
+        ends = pr[i, TOK:].astype(F32)
+        ends = jnp.concatenate([ends[:, 0:TOK - 128], ends[:, TOK - 128:]], axis=0)
+        whole_of.append(jnp.concatenate([pr[i, 0:TOK].astype(F32), ends], axis=1))
     merged = []
     for row, rate, lo, hi in ((0, RATE_B, 0, VB), (2, RATE_A, VB, VB + VA)):
         tops = [sr[i, row:row + 1, :] for i in range(NX)]
         top = functools.reduce(jnp.maximum, tops)
         part = [jnp.exp2((tops[i] - top) * rate) * sr[i, row + 1:row + 2, :] for i in range(NX)]
         whole = 1.0 / sum(part)
-        merged.append(sum(pr[i, lo:hi].astype(F32) * (part[i] * whole) for i in range(NX)))
+        merged.append(sum(whole_of[i][lo:hi] * (part[i] * whole) for i in range(NX)))
     turned = jnp.concatenate(merged, axis=0).astype(BF16)
     heads[...] = nt(unit_tok, turned).astype(BF16)
 
@@ -433,6 +439,10 @@
     f_s[...] = fdot(place, hs[...]).reshape(NSP, CAPP, W).astype(BF16)
     f_r[sp] = f_s[sp]
 
+    def far_first(i):
+        odd = lax.rem(i, 2)
+        return NSP // 2 + odd * ((i + 1) // 2) - (1 - odd) * (i // 2)
+
     def sp_copy(k, src, dst, ss, rs, to):
         peer = lax.rem(sp + k, NSP) if to else lax.rem(sp + NSP - k, NSP)
         return rcopy(src.at[peer], dst.at[sp if to else peer], ss.at[k], rs.at[k], sdev(peer))
@@ -445,7 +455,7 @@
         sp_copy(k, f_s, f_r, f_ss, f_rs, False).wait()
         return 0
 
-    lax.fori_loop(1, NSP, f_send, 0)
+    lax.fori_loop(0, NSP - 1, lambda i, _: f_send(far_first(i), 0), 0)
 
     hidden[:, lanes(t, W)] = hs[...]
 
@@ -493,7 +503,7 @@
         e_got(4).wait_recv()
         f2_s[...] = fdot(place, hidden[:, lanes(t4, W)]).reshape(NSP, CAPP, W).astype(BF16)
         f2_r[sp] = f2_s[sp]
-        lax.fori_loop(1, NSP, f2_send, 0)
+        lax.fori_loop(0, NSP - 1, lambda i, _: f2_send(far_first(i), 0), 0)
         e_fwd(4, c).start()
         for off in (1, 7, 2, 6, 3, 5):
             e_got(off).wait_recv()
@@ -576,7 +586,7 @@
         sp_copy(k, f2_s, j2_r, j2_ss, j2_rs, False).wait()
         return 0
 
-    lax.fori_loop(1, NSP, j2_send, 0)
+    lax.fori_loop(0, NSP - 1, lambda i, _: j2_send(far_first(i), 0), 0)
     i_wait(2, 6)
     i_step(2)
     i_pair(1)
@@ -605,7 +615,7 @@
         sp_copy(k, f_s, j_r, j_ss, j_rs, False).wait()
         return 0
 
-    lax.fori_loop(1, NSP, j_send, 0)
+    lax.fori_loop(0, NSP - 1, lambda i, _: j_send(far_first(i), 0), 0)
     scatter_send((3, 5, 1, 7, 0), own_s, po_s, pi_s, sb_s, rb_s, ps_ss, ps_rs, s_ss, s_rs, mg_s, ms_ss, ms_rs)
     rows8 = jnp.concatenate(
         [slot_row(0).astype(F32), slot_row(1).astype(F32), rw_t[0:1, :], rw_t[1:2, :], jnp.zeros((4, TOK), F32)], axis=0
@@ -664,7 +674,8 @@
             for d in range(2):
                 i_copy(d, k, h).wait_send()
     lax.fori_loop(1, NTP, l_wait, 0)
-    out[...] = (l_r[0:OWN, :].astype(F32) + l2_r[0:OWN, :].astype(F32)).astype(BF16)
+    out_near[...] = l_r[0:OWN, :]
+    out_far[...] = l2_r[0:OWN, :]
 
 
 def layer(vmem_args, hbm_args):
@@ -674,8 +685,8 @@
     zsem, ysem = (2, 4, Z_PIECES), (2, 4, PIECES)
     scratch = [
         vm((NZ, TOK, 640), BF16), vm((NX, TOK, 256), BF16), vm((VA + VB, 512), BF16), row, row, row, row,
-        vm((VA, NX * TOK), F32), vm((VB, NX * TOK), F32), vm((NX, VA + VB, TOK), BF16), vm((NX, 8, TOK), F32),
-        vm((NX, VA + VB, TOK), BF16), vm((NX, 8, TOK), F32), vm((TOK, VA + VB), BF16), vm((TOK, 8), F32),
+        vm((VA, NX * TOK), F32), vm((VB, NX * TOK), F32), vm((NX, TOK + TOK // 2, 128), BF16), vm((NX, 8, TOK), F32),
+        vm((NX, TOK + TOK // 2, 128), BF16), vm((NX, 8, TOK), F32), vm((TOK, VA + VB), BF16), vm((TOK, 8), F32),
         vm((VA + VB, D), BF16), vm((D, 2 * W), BF16), vm((W, D), BF16), vm((D, 2 * W), BF16), vm((W, D), BF16),
         vm((OWNP, D), BF16), vm((NTP, OWNP, W), BF16),
         vm((NY, TOK, W), F32), vm((NY, TOK, W), BF16), vm((NY, TOK, W), BF16), vm((NY, TOK, W), BF16), vm((NY, TOK, W), BF16),
@@ -698,15 +709,16 @@
     ] + [dma, dma]
     vspec = pl.BlockSpec(memory_space=pltpu.VMEM)
     hspec = pl.BlockSpec(memory_space=pl.ANY)
-    return pl.pallas_call(
+    near, far = pl.pallas_call(
         layer_kernel,
-        out_shape=jax.ShapeDtypeStruct((OWN, D), BF16),
+        out_shape=[jax.ShapeDtypeStruct((OWN, D), BF16)] * 2,
         in_specs=[vspec] * len(vmem_args) + [hspec] * len(hbm_args),
-        out_specs=vspec,
+        out_specs=[vspec] * 2,
         scratch_shapes=scratch,
         compiler_params=pltpu.CompilerParams(collective_id=1, has_side_effects=True, vmem_limit_bytes=60 * 2**20),
         name="layer",
     )(*vmem_args, *hbm_args)
+    return (near.astype(F32) + far.astype(F32)).astype(BF16)
 
 
 def tables(positions):

time: 118 us -> 117 us (level)
  Pallas kernels: 116 us -> 114 us
  other arithmetic: 0.79 us -> 2.32 us
  local copies, waits for them, and re-layouts: 1.47 us -> 0 us
    convert_element_type x0 -> x1, other arithmetic: none -> 1.52 us  [layer(): return (near.astype(F32) + far.astype(F32)).astype(BF16)]
    unnamed x1 -> x0, local copies, waits for them, and re-layouts: 1.47 us -> none
    pallas_call x1, Pallas kernels: 116 us -> 114 us  [layer(): pl.pallas_call(layer_kernel, out_shape=[jax.ShapeDtypeStruct((OWN, D), BF...]
where the time goes in v5:
time: 117 us
  Pallas kernels  114 us (97%)
  other arithmetic  2.32 us (2%)
    pallas_call x1, Pallas kernels, layer(): pl.pallas_call(layer_kernel, out_shape=[jax.ShapeDtypeStruct((OWN, D), BF...  114 us

profile of v5, /device:TPU:1, one launch (start us, length us, event | category | flops | bytes accessed | tf_op | source)
XLA Modules:
  0.0 116.8 jit_solution(8494495523226240232)
XLA Ops:
  0.0 0.1 fusion
  0.2 0.6 pad_maximum_fusion
  0.8 114.5 %layer.1 = (bf16[12,2048]{1,0:T(8,128)(2,1)}, bf16[12,2048]{1,0:T(8,128)(2,1)}) custom-call(bf16[192,96]{1,0:T(8,128)(2,1)} %qa.1, bf16[160,192]{1,0:T(8,128)(2,1)} %bitcast.13, bf16[192,512]{1,0:T(8,128)(2,1)} %lat.1, bf16[32,192]{1,0:T(8,128)(2,1)} %bitcast.16, f32[32,192]{1,0:T(8,128)} %get-tuple-element.12.cosine, f32[32,192]{1,0:T(8,128)} %get-tuple-element.13.sine, ...), custom_call_target="tpu_custom_call" | custom-call | tf_op jit(solution)/shard_map/layer/pallas_call | solution.py:712
  115.3 1.5 %add_convert_fusion = bf16[12,2048]{1,0:T(8,128)(2,1)} fusion(bf16[12,2048]{1,0:T(8,128)(2,1)} %get-tuple-element.8, bf16[12,2048]{1,0:T(8,128)(2,1)} %get-tuple-element.7), kind=kLoop, calls=%fused_computation | loop fusion | flops 98304 | bytes 147456 | tf_op jit(solution)/shard_map/convert_element_type | solution.py:721
  (2 shorter events, 0.0 us)
